TPU v7x, 256 devices: a whole 4x4x8 slice. The times are simulated.
256 devices in a mesh: rep: 2 (over z_hi), fs: 16 (over z_lo, x), tp: 8 (over y, core).
Axes of the slice: x: 4, y: 4, z: 8 (z_hi: 2, z_lo: 4; z = z_hi * 4 + z_lo), core: 2. Of those that a mesh axis runs over, the one named last changes fastest.
Arguments:
- tokens: bfloat16 [32768, 2048], P(('rep', 'fs', 'tp')), may hold values from -6 to 6
- norm1_gain: float32 [2048], replicated, may hold values from 0.1 to 1.9
- in_weight: bfloat16 [2048, 1024], P('fs', 'tp'), may hold values from -0.125 to 0.125
- group_weight: bfloat16 [8, 128, 128], P('tp'), may hold values from -0.5 to 0.5
- pool_scale: float32 [1024], P('tp'), may hold values from 0.1 to 1.9
- out_weight: bfloat16 [1024, 2048], P('tp', 'fs'), may hold values from -0.1875 to 0.1875
- norm2_gain: float32 [2048], replicated, may hold values from 0.1 to 1.9
- up_weight: bfloat16 [2048, 8192], P('fs', 'tp'), may hold values from -0.125 to 0.125
- down_weight: bfloat16 [8192, 2048], P('tp', 'fs'), may hold values from -0.0625 to 0.0625
Outputs:
- layer_out: bfloat16 [32768, 2048], P(('rep', 'fs', 'tp'))
All inputs are finite; a program needn't handle non-finite values.
Results may differ from a plain program's by a relative error of at most 0.02.
Values may be sent and summed in bfloat16 or wider, within the bound.
A program may use at most 128 MiB of HBM per device.

v0:
```python
import jax
import jax.numpy as jnp
from jax import lax
from jax.sharding import Mesh
from jax.sharding import PartitionSpec as P

GROUP_DIM = 128
TP = ("tp_0", "tp_1")
FS = ("fs_0", "fs_1")
REP_FS_TP = ("rep", "fs_0", "fs_1", "tp_0", "tp_1")


epsilon = 1e-06


def laid_out(pieces, dim):
    dims = list(pieces.shape[1:])
    dims[dim] *= pieces.shape[0]
    return jnp.moveaxis(pieces, 0, dim).reshape(dims)


def copy_for_each(x, axis):
    peers = lax.axis_size(axis)
    return lax.all_to_all(jnp.broadcast_to(x[None], (peers, *x.shape)), axis, 0, 0, tiled=True)


def collect(x, axis, dim):
    return laid_out(copy_for_each(x, axis), dim)


def gather_axes(x, axes, dim):
    far, near = axes
    pieces = copy_for_each(copy_for_each(x, far), near)
    return laid_out(pieces.swapaxes(0, 1).reshape(-1, *x.shape), dim)


def all_blocks(x, axes, order):
    pieces = x
    for k in order:
        pieces = lax.all_gather(pieces, axes[k])
    done = order[::-1]
    back = [done.index(k) for k in range(len(axes))]
    pieces = pieces.transpose(*back, *range(len(axes), pieces.ndim))
    return pieces.reshape(-1, *x.shape)


def whole_of(x, axes, order, dim):
    return laid_out(all_blocks(x, axes, order), dim)


def cut_along(x, dim, peers):
    dims = x.shape
    pieces = x.reshape(*dims[:dim], peers, dims[dim] // peers, *dims[dim + 1 :])
    return jnp.moveaxis(pieces, dim, 0)


def sum_at_owner(x, axis, dim):
    pieces = cut_along(x, dim, lax.axis_size(axis))
    arrived = lax.all_to_all(pieces, axis, split_axis=0, concat_axis=0, tiled=True)
    return arrived.astype(jnp.float32).sum(axis=0)


def summed_rows(x, axes, dim):
    far, near = axes
    pieces = cut_along(x, dim, lax.axis_size(far))
    nearer = sum_at_owner(pieces, near, dim + 1)
    arrived = lax.all_to_all(
        nearer.astype(jnp.bfloat16), far, split_axis=0, concat_axis=0, tiled=True
    )
    return arrived.astype(jnp.float32).sum(axis=0)


def rms_norm(values, gain):
    scale = lax.rsqrt(jnp.mean(values * values, axis=-1, keepdims=True) + epsilon)
    return values * scale * gain


def shifted(values, offset):
    return jnp.pad(values, ((offset, 0), (0, 0)))[: values.shape[0]]


def mix_groups(projected, group_weight, pool_scale):
    length = projected.shape[0]
    local_groups = group_weight.shape[0]
    values = projected.astype(jnp.float32)
    level_sums = []
    running = values
    offset = 1
    for level in range(4):
        running = running + shifted(running, offset)
        offset = offset * 2
        level_sums.append(running)
    first_group = lax.axis_index(TP) * local_groups
    group_level = (first_group + jnp.arange(local_groups, dtype=jnp.int32)) % 4
    column_level = jnp.repeat(group_level, GROUP_DIM)[None, :]
    position = jnp.arange(length, dtype=jnp.int32)[:, None]
    window_mean = jnp.zeros_like(values)
    for level in range(4):
        count = jnp.minimum(position + 1, 2 ** (level + 1)).astype(jnp.float32)
        window_mean = jnp.where(column_level == level, level_sums[level] / count, window_mean)
    pooled = (window_mean - values).astype(jnp.bfloat16).reshape(length, local_groups, GROUP_DIM)
    mapped = jnp.einsum("sgc,gcd->sgd", pooled, group_weight, preferred_element_type=jnp.float32)
    return (mapped.reshape(length, local_groups * GROUP_DIM) * pool_scale).astype(jnp.bfloat16)


def local(
    tokens,
    norm1_gain,
    in_weight,
    group_weight,
    pool_scale,
    out_weight,
    norm2_gain,
    up_weight,
    down_weight,
):
    stream = tokens.astype(jnp.float32)
    normed = rms_norm(stream, norm1_gain).astype(jnp.bfloat16)
    in_local = collect(in_weight, FS, 0)
    projected = jnp.dot(
        gather_axes(normed, ("tp_0", "tp_1"), 0), in_local, preferred_element_type=jnp.float32
    ).astype(jnp.bfloat16)
    pool_out = mix_groups(projected, group_weight, pool_scale)
    out_local = collect(out_weight, FS, 1)
    block_rows = pool_out
    mixed = lax.psum_scatter(
        jnp.dot(block_rows, out_local, preferred_element_type=jnp.float32).astype(jnp.bfloat16),
        TP,
        scatter_dimension=0,
        tiled=True,
    ).astype(jnp.float32)
    mixed_stream = stream + mixed
    normed_two = rms_norm(mixed_stream, norm2_gain).astype(jnp.bfloat16)
    up_local = whole_of(up_weight, FS, (0, 1), 0)
    upper = jnp.dot(
        gather_axes(normed_two, ("tp_0", "tp_1"), 0), up_local, preferred_element_type=jnp.float32
    )
    hidden = jnp.square(jax.nn.relu(upper)).astype(jnp.bfloat16)
    down_local = whole_of(down_weight, FS, (0, 1), 1)
    block_rows = hidden
    channel_sum = summed_rows(
        jnp.dot(block_rows, down_local, preferred_element_type=jnp.float32).astype(jnp.bfloat16),
        ("tp_0", "tp_1"),
        0,
    )
    return (mixed_stream + channel_sum).astype(jnp.bfloat16)


def solution(mesh):
    split = Mesh(
        mesh.devices.reshape(mesh.shape["rep"], 4, 4, 4, 2), ("rep", "fs_0", "fs_1", "tp_0", "tp_1")
    )
    in_specs = (
        P(REP_FS_TP, None),
        P(),
        P(FS, TP),
        P(TP, None, None),
        P(TP),
        P(TP, FS),
        P(),
        P(FS, TP),
        P(TP, FS),
    )
    out_specs = P(REP_FS_TP, None)
    return jax.shard_map(local, mesh=split, in_specs=in_specs, out_specs=out_specs, check_vma=False)
```

profile of v0, /device:TPU:1, one launch (start us, length us, event | category | flops | bytes accessed | tf_op | source)
XLA Modules:
  0.0 296.8 jit_solution(17428534109054152033)
XLA Ops:
  7.4 1.2 fusion.4
  8.6 1.2 fusion.6
  9.9 1.6 broadcast_in_dim.70
  11.5 5.0 %all-to-all-start = ((bf16[4,128,2048]{2,1,0:T(8,128)(2,1)}), bf16[4,128,2048]{2,1,0:T(8,128)(2,1)S(1)}, u32[]{:S(2)}, u32[]{:S(2)}) async-start(bf16[4,128,2048]{2,1,0:T(8,128)(2,1)} %broadcast_in_dim.70), calls=%async_computation | async-start | bytes 4194304 | tf_op jit(solution)/shard_map/all_to_all | solution.py:24
  16.5 0.7 all-gather.13.cloned.1.call-update
  17.2 23.9 %all-to-all-done = bf16[4,128,2048]{2,1,0:T(8,128)(2,1)S(1)} async-done(((bf16[4,128,2048]{2,1,0:T(8,128)(2,1)}), bf16[4,128,2048]{2,1,0:T(8,128)(2,1)S(1)}, u32[]{:S(2)}, u32[]{:S(2)}) %all-to-all-start) | async-done | bytes 2097184 | tf_op jit(solution)/shard_map/all_to_all | solution.py:24
  41.1 0.5 broadcast_in_dim.71
  41.7 10.6 %all_to_all.40 = bf16[2,4,128,2048]{3,2,1,0:T(8,128)(2,1)} all-to-all(bf16[2,4,128,2048]{3,2,1,0:T(8,128)(2,1)S(1)} %broadcast_in_dim.71), channel_id=1, replica_groups=mesh['rep'=2,'fs_0'=4,'fs_1'=4,'tp_0'=4,'tp_1'=2] {'tp_1'}, dimensions={0} | all-to-all | bytes 8388608 | tf_op jit(solution)/shard_map/all_to_all | solution.py:24
  52.2 0.9 broadcast_in_dim.72
  53.1 8.2 %all-to-all-start.2 = ((bf16[16,128,128]{2,1,0:T(8,128)(2,1)}), bf16[16,128,128]{2,1,0:T(8,128)(2,1)S(1)}, u32[]{:S(2)}, u32[]{:S(2)}) async-start(bf16[16,128,128]{2,1,0:T(8,128)(2,1)} %broadcast_in_dim.72), calls=%async_computation.2 | async-start | bytes 1048576 | tf_op jit(solution)/shard_map/all_to_all | solution.py:24
  61.3 0.0 all-gather.9.cloned.1.call-start
  61.4 0.7 all-gather.9.cloned.1.call-update
  62.1 0.1 copy.24
  62.2 4.8 %copy.23 = bf16[2,4,128,2048]{3,2,0,1:T(8,128)(2,1)} copy(bf16[2,4,128,2048]{3,2,1,0:T(8,128)(2,1)} %all_to_all.40) | data formatting | bytes 8388608 | tf_op jit(solution)/shard_map/all_to_all | solution.py:24
  67.0 8.4 %all-to-all-done.2 = bf16[16,128,128]{2,1,0:T(8,128)(2,1)S(1)} async-done(((bf16[16,128,128]{2,1,0:T(8,128)(2,1)}), bf16[16,128,128]{2,1,0:T(8,128)(2,1)S(1)}, u32[]{:S(2)}, u32[]{:S(2)}) %all-to-all-start.2) | async-done | bytes 524320 | tf_op jit(solution)/shard_map/all_to_all | solution.py:24
  75.4 0.9 broadcast_in_dim.77
  76.3 4.9 %all-to-all-start.3 = ((bf16[16,128,128]{1,2,0:T(8,128)(2,1)}), bf16[16,128,128]{1,2,0:T(8,128)(2,1)S(1)}, u32[]{:S(2)}, u32[]{:S(2)}) async-start(bf16[16,128,128]{1,2,0:T(8,128)(2,1)} %broadcast_in_dim.77), calls=%async_computation.3 | async-start | bytes 1048576 | tf_op jit(solution)/shard_map/all_to_all | solution.py:24
  81.3 0.0 reduce-scatter.2.cloned.1.call-start
  81.3 3.5 %fusion.2 = f32[1024,128]{1,0:T(8,128)S(1)} fusion(bf16[1024,2048]{1,0:T(8,128)(2,1)} %bitcast.60, bf16[2048,128]{1,0:T(8,128)(2,1)S(1)} %bitcast.69), kind=kOutput, calls=%fused_computation.12 | convolution fusion | flops 537133056 | bytes 5242880 | tf_op jit(solution)/shard_map/dot_general | solution.py:120
  84.8 0.1 fusion.7
  84.9 0.1 fusion.8
  84.9 0.1 fusion.9
  85.0 19.3 %all-to-all-done.3 = bf16[16,128,128]{1,2,0:T(8,128)(2,1)S(1)} async-done(((bf16[16,128,128]{1,2,0:T(8,128)(2,1)}), bf16[16,128,128]{1,2,0:T(8,128)(2,1)S(1)}, u32[]{:S(2)}, u32[]{:S(2)}) %all-to-all-start.3) | async-done | bytes 524320 | tf_op jit(solution)/shard_map/all_to_all | solution.py:24
  104.3 3.6 %convolution_convert_fusion = bf16[1024,2048]{1,0:T(8,128)(2,1)} fusion(bf16[128,2048]{0,1:T(8,128)(2,1)S(1)} %bitcast.72, f32[1024,128]{1,0:T(8,128)S(1)} %fusion.2, f32[1024,128]{1,0:T(8,128)S(1)} %fusion.7, f32[1024,128]{1,0:T(8,128)S(1)} %fusion.9, f32[128]{0:T(128)S(1)} %copy-done.7, f32[1024]{0:T(1024)S(1)} %get-tuple-element.5, ...), kind=kOutput, calls=%fused_computation.3 | convolution fusion | flops 574357504 | bytes 6341124 | tf_op jit(solution)/shard_map/dot_general | solution.py:127
  107.9 0.0 all-gather.15.cloned.1.call-start
  108.0 0.7 all-gather.15.cloned.1.call-update
  108.6 0.0 all-gather.11.cloned.1.call-start
  108.7 0.5 all-gather.11.cloned.1.call-update
  109.2 38.3 %reduce-scatter.2.cloned.1.call-done = bf16[128,2048]{1,0:T(8,128)(2,1)} async-done(((bf16[1024,2048]{1,0:T(8,128)(2,1)}), bf16[128,2048]{1,0:T(8,128)(2,1)}) %reduce-scatter.2.cloned.1.call-update) | async-done | bytes 524304 | tf_op jit(solution)/shard_map/reduce_scatter | solution.py:126
  147.5 1.3 multiply_reduce_fusion
  148.9 1.3 multiply_convert_fusion.1
  150.1 1.6 broadcast_in_dim.78
  151.7 5.3 %all-to-all-start.4 = ((bf16[4,128,2048]{2,1,0:T(8,128)(2,1)}), bf16[4,128,2048]{2,1,0:T(8,128)(2,1)S(1)}, u32[]{:S(2)}, u32[]{:S(2)}) async-start(bf16[4,128,2048]{2,1,0:T(8,128)(2,1)} %broadcast_in_dim.78), calls=%async_computation.5 | async-start | bytes 4194304 | tf_op jit(solution)/shard_map/all_to_all | solution.py:24
  157.1 5.3 %all-gather.15.cloned.1.call-done = bf16[16,1024,128]{2,1,0:T(8,128)(2,1)} async-done(((bf16[4,1024,128]{2,1,0:T(8,128)(2,1)}), bf16[16,1024,128]{2,1,0:T(8,128)(2,1)}) %all-gather.15.cloned.1.call-update) | async-done | bytes 4194320 | tf_op jit(solution)/shard_map/all_gather | solution.py:40
  162.4 4.5 %copy.27 = bf16[4,4,1024,128]{3,2,1,0:T(8,128)(2,1)} copy(bf16[4,4,1024,128]{3,2,0,1:T(8,128)(2,1)} %bitcast.63) | data formatting | bytes 8388608 | tf_op jit(solution)/shard_map/transpose | solution.py:43
  166.9 6.4 %copy.28 = bf16[1024,16,128]{0,2,1:T(8,128)(2,1)} copy(bf16[1024,16,128]{2,0,1:T(8,128)(2,1)} %bitcast.61) | data formatting | bytes 8388608 | tf_op jit(solution)/shard_map/transpose | solution.py:19
  173.3 41.8 %all-gather.11.cloned.1.call-done = bf16[16,128,1024]{2,1,0:T(8,128)(2,1)} async-done(((bf16[4,128,1024]{2,1,0:T(8,128)(2,1)}), bf16[16,128,1024]{2,1,0:T(8,128)(2,1)}) %all-gather.11.cloned.1.call-update) | async-done | bytes 4194320 | tf_op jit(solution)/shard_map/all_gather | solution.py:40
  215.2 4.8 %copy.26 = bf16[4,4,128,1024]{3,2,1,0:T(8,128)(2,1)} copy(bf16[4,4,128,1024]{3,2,0,1:T(8,128)(2,1)} %bitcast.64) | data formatting | bytes 8388608 | tf_op jit(solution)/shard_map/transpose | solution.py:43
  219.9 0.5 broadcast_in_dim.79
  220.5 7.6 %all_to_all.41 = bf16[2,4,128,2048]{3,2,1,0:T(8,128)(2,1)S(1)} all-to-all(bf16[2,4,128,2048]{3,2,1,0:T(8,128)(2,1)S(1)} %broadcast_in_dim.79), channel_id=1, replica_groups=mesh['rep'=2,'fs_0'=4,'fs_1'=4,'tp_0'=4,'tp_1'=2] {'tp_1'}, dimensions={0} | all-to-all | bytes 8388608 | tf_op jit(solution)/shard_map/all_to_all | solution.py:24
  228.0 2.3 copy.25
  230.3 14.4 %convolution_convert_fusion.1 = bf16[1024,2048]{1,0:T(8,128)(2,1)} fusion(bf16[1024,2048]{0,1:T(8,128)(2,1)} %bitcast.65, bf16[1024,2048]{1,0:T(8,128)(2,1)} %bitcast.67, bf16[2048,1024]{1,0:T(8,128)(2,1)} %bitcast.66), kind=kOutput, calls=%fused_computation.4 | convolution fusion | flops 8595177472 | bytes 16777216 | tf_op jit(solution)/shard_map/dot_general | solution.py:142
  244.7 2.5 copy.31
  247.2 8.2 %all_to_all.42 = bf16[2,4,128,2048]{3,2,1,0:T(8,128)(2,1)} all-to-all(bf16[2,4,128,2048]{3,2,1,0:T(8,128)(2,1)S(1)} %bitcast.62), channel_id=1, replica_groups=mesh['rep'=2,'fs_0'=4,'fs_1'=4,'tp_0'=4,'tp_1'=2] {'tp_1'}, dimensions={0} | all-to-all | bytes 8388608 | tf_op jit(solution)/shard_map/all_to_all | solution.py:59
  255.3 3.6 %reduce_sum.41 = bf16[4,128,2048]{2,1,0:T(8,128)(2,1)S(1)} reduce(bf16[2,4,128,2048]{3,2,1,0:T(8,128)(2,1)} %all_to_all.42, bf16[]{:T(256)} %constant.62.clone.1), dimensions={0}, to_apply=%region_3.4 | reduce | flops 1048576 | bytes 6291458 | tf_op jit(solution)/shard_map/reduce_sum | solution.py:60
  258.9 29.4 %all_to_all.43 = bf16[4,128,2048]{2,1,0:T(8,128)(2,1)S(1)} all-to-all(bf16[4,128,2048]{2,1,0:T(8,128)(2,1)S(1)} %reduce_sum.41), channel_id=1, replica_groups=mesh['rep'=2,'fs_0'=4,'fs_1'=4,'tp_0'=4,'tp_1'=2] {'tp_0'}, dimensions={0} | all-to-all | bytes 4194304 | tf_op jit(solution)/shard_map/all_to_all | solution.py:67
  288.3 0.4 convert_reduce_fusion
  288.7 1.0 add_convert_fusion
  (25 shorter events, 0.1 us)
Async XLA Ops:
  7.4 96.9 %copy-start = (bf16[1,128,128]{2,1,0:T(8,128)(2,1)S(1)}, bf16[1,128,128]{2,1,0:T(8,128)(2,1)}, u32[]{:S(2)}) copy-start(bf16[1,128,128]{2,1,0:T(8,128)(2,1)} %param.12) | copy-start | bytes 98308
  11.5 29.7 %all-to-all-start = ((bf16[4,128,2048]{2,1,0:T(8,128)(2,1)}), bf16[4,128,2048]{2,1,0:T(8,128)(2,1)S(1)}, u32[]{:S(2)}, u32[]{:S(2)}) async-start(bf16[4,128,2048]{2,1,0:T(8,128)(2,1)} %broadcast_in_dim.70), calls=%async_computation | async-start | bytes 4194304 | tf_op jit(solution)/shard_map/all_to_all | solution.py:24
  16.5 91.5 %all-gather.13.cloned.1.call-start = ((), (), s32[]{:S(2)}) async-start(), calls=%async_computation.12 | async-start | bytes 1310720 | tf_op jit(solution)/shard_map/all_gather | solution.py:40
  41.6 10.6 %copy-start.4 = (bf16[128,128]{1,0:T(8,128)(2,1)S(1)}, bf16[128,128]{1,0:T(8,128)(2,1)}, u32[]{:S(2)}) copy-start(bf16[128,128]{1,0:T(8,128)(2,1)} %param.11) | copy-start | bytes 98308
  41.6 20.5 %copy-start.5 = (bf16[128,128]{1,0:T(8,128)(2,1)S(1)}, bf16[128,128]{1,0:T(8,128)(2,1)}, u32[]{:S(2)}) copy-start(bf16[128,128]{1,0:T(8,128)(2,1)} %param.14) | copy-start | bytes 98308
  53.1 22.3 %all-to-all-start.2 = ((bf16[16,128,128]{2,1,0:T(8,128)(2,1)}), bf16[16,128,128]{2,1,0:T(8,128)(2,1)S(1)}, u32[]{:S(2)}, u32[]{:S(2)}) async-start(bf16[16,128,128]{2,1,0:T(8,128)(2,1)} %broadcast_in_dim.72), calls=%async_computation.2 | async-start | bytes 1048576 | tf_op jit(solution)/shard_map/all_to_all | solution.py:24
  61.3 47.4 %all-gather.9.cloned.1.call-start = ((), (), s32[]{:S(2)}) async-start(), calls=%async_computation.10 | async-start | bytes 1310720 | tf_op jit(solution)/shard_map/all_gather | solution.py:40
  76.3 28.0 %all-to-all-start.3 = ((bf16[16,128,128]{1,2,0:T(8,128)(2,1)}), bf16[16,128,128]{1,2,0:T(8,128)(2,1)S(1)}, u32[]{:S(2)}, u32[]{:S(2)}) async-start(bf16[16,128,128]{1,2,0:T(8,128)(2,1)} %broadcast_in_dim.77), calls=%async_computation.3 | async-start | bytes 1048576 | tf_op jit(solution)/shard_map/all_to_all | solution.py:24
  81.3 66.3 %reduce-scatter.2.cloned.1.call-start = ((), (), s32[]{:S(2)}) async-start(), calls=%async_computation.9 | async-start | bytes 4718592 | tf_op jit(solution)/shard_map/reduce_scatter | solution.py:126
  81.3 23.0 %copy-start.7 = (f32[128]{0:T(128)S(1)}, f32[128]{0:T(128)}, u32[]{:S(2)}) copy-start(f32[128]{0:T(128)} %param.13) | copy-start | bytes 1540
  107.9 39.7 %copy-start.2 = (bf16[128,2048]{1,0:T(8,128)(2,1)S(1)}, bf16[128,2048]{1,0:T(8,128)(2,1)}, u32[]{:S(2)}) copy-start(bf16[128,2048]{1,0:T(8,128)(2,1)} %param.9) | copy-start | bytes 1572868
  107.9 41.0 %copy-start.6 = (f32[2048]{0:T(1024)S(1)}, f32[2048]{0:T(1024)}, u32[]{:S(2)}) copy-start(f32[2048]{0:T(1024)} %param.15) | copy-start | bytes 24580
  107.9 54.5 %all-gather.15.cloned.1.call-start = ((), (), s32[]{:S(2)}) async-start(), calls=%async_computation.13 | async-start | bytes 5242880 | tf_op jit(solution)/shard_map/all_gather | solution.py:40
  108.6 106.6 %all-gather.11.cloned.1.call-start = ((), (), s32[]{:S(2)}) async-start(), calls=%async_computation.11 | async-start | bytes 5242880 | tf_op jit(solution)/shard_map/all_gather | solution.py:40
  151.7 68.2 %all-to-all-start.4 = ((bf16[4,128,2048]{2,1,0:T(8,128)(2,1)}), bf16[4,128,2048]{2,1,0:T(8,128)(2,1)S(1)}, u32[]{:S(2)}, u32[]{:S(2)}) async-start(bf16[4,128,2048]{2,1,0:T(8,128)(2,1)} %broadcast_in_dim.78), calls=%async_computation.5 | async-start | bytes 4194304 | tf_op jit(solution)/shard_map/all_to_all | solution.py:24
  255.3 34.4 %copy-start.1 = (bf16[1,128,128]{2,1,0:T(8,128)(2,1)S(1)}, bf16[1,128,128]{2,1,0:T(8,128)(2,1)}, u32[]{:S(2)}) copy-start(bf16[1,128,128]{2,1,0:T(8,128)(2,1)} %param.12) | copy-start | bytes 98308
  258.9 29.8 %copy-start.3 = (bf16[128,2048]{1,0:T(8,128)(2,1)S(1)}, bf16[128,2048]{1,0:T(8,128)(2,1)}, u32[]{:S(2)}) copy-start(bf16[128,2048]{1,0:T(8,128)(2,1)} %reduce-scatter.2.cloned.1.call-done) | copy-start | bytes 1572868
Sparse Core Ops, SparseCore 0:
  19.1 36.3 all-gather.12
  63.9 39.7 all-gather.8
  110.5 51.8 all-gather.14
  164.0 51.0 all-gather.10
Sparse Core Ops, SparseCore 1:
  108.0 39.5 reduce-scatter.1
where the time goes:
time: 298 us; the launch traced here: 297 us
  waiting for transfers between devices  140 us (47%)
  blocking collectives  55.7 us (19%)
  local copies, waits for them, and re-layouts  31.4 us (11%)
  starting transfers between devices  23.6 us (8%)
  matrix products  21.4 us (7%)
  between operations  14.8 us (5%)
  other arithmetic  10.2 us (3%)
    all_to_all x4, waiting for transfers between devices, copy_for_each(): lax.all_to_all(jnp.broadcast_to(x[None], (peers, *x.shape)), axis, 0, 0,...  51.7 us
    all_gather x4, waiting for transfers between devices, all_blocks(): pieces = lax.all_gather(pieces, axes[k])  47.2 us
    reduce_scatter x1, waiting for transfers between devices, local(): lax.psum_scatter(jnp.dot(block_rows, out_local, preferred_element_type=jn...  38.3 us
    all_to_all x1, blocking collectives, summed_rows(): lax.all_to_all(nearer.astype(jnp.bfloat16), far, split_axis=0, concat_axi...  29.4 us
    all_to_all x4, starting transfers between devices, copy_for_each(): lax.all_to_all(jnp.broadcast_to(x[None], (peers, *x.shape)), axis, 0, 0,...  23.5 us
    all_to_all x2, blocking collectives, copy_for_each(): lax.all_to_all(jnp.broadcast_to(x[None], (peers, *x.shape)), axis, 0, 0,...  18.1 us
    dot_general x1, matrix products, local(): jnp.dot(block_rows, down_local, preferred_element_type=jnp.float32)  14.4 us
    transpose x2, local copies, waits for them, and re-layouts, all_blocks(): pieces = pieces.transpose(*back, *range(len(axes), pieces.ndim))  9.27 us
  transfers between devices with their start and end apart: 9, of which 6 were waited for; matrix products, arithmetic and copies ran while one was open for 12% of the time, Pallas kernels for 0%

commit v1 on v0

v1 whole, which is shorter than its diff:
```python
import functools

import jax
import jax.numpy as jnp
from jax import lax
from jax.experimental import pallas as pl
from jax.experimental.pallas import tpu as pltpu
from jax.sharding import PartitionSpec as P

EPS = 1e-06
MESH = pl.DeviceIdType.MESH
F32 = jnp.float32
BF16 = jnp.bfloat16
HALO = 16
ROWS = 128
EXT = HALO + ROWS
ORDER = (0, 3, 1, 2)

PER_MATRIX = 36
MIX, UP, DOWN = 0, 1, 2
Y_BASE = 3 * PER_MATRIX
HALO_K = Y_BASE + 16
AG_BASE = Y_BASE + 17
RS_BASE = AG_BASE + 6
N_SEMS = RS_BASE + 32


def kernel(
    tokens_hbm, gain1, in_hbm, group_hbm, scale_hbm, out_hbm, gain2, up_hbm, down_hbm,
    o_ref,
    tok, mixw, upw, downw, groupw, scales,
    normed, acc, mixed, pool, gathered, hidden,
    far_out, far_in, near_out, near_in, keep,
    send_sem, recv_sem, load_sem,
):
    rep = lax.axis_index("rep")
    fs = lax.axis_index("fs")
    tp = lax.axis_index("tp")
    x = lax.rem(fs, 4)
    zlo = lax.div(fs, 4)
    z = rep * 4 + zlo
    y = lax.div(tp, 2)
    core = lax.rem(tp, 2)
    other = 1 - core

    def at(x_, z_, tp_):
        return (lax.div(z_, 4), lax.rem(z_, 4) * 4 + x_, tp_)

    def step(first_axis, d):
        on_x = other if first_axis else core
        on_z = core if first_axis else other
        return at(lax.rem(x + on_x * d + 4, 4), lax.rem(z + on_z * d + 8, 8), tp)

    a_plus, a_minus = step(True, 1), step(True, -1)
    b_plus, b_minus = step(False, 1), step(False, -1)
    partner = (rep, fs, y * 2 + other)

    def on_y(d, c):
        return (rep, fs, lax.rem(y + d + 4, 4) * 2 + c)

    y_plus, y_minus, y_far = on_y(1, core), on_y(-1, core), on_y(2, core)
    neighbours = (
        a_plus, a_minus, b_plus, b_minus, partner, y_plus, y_minus, y_far,
        on_y(1, other), on_y(-1, other),
    )

    loads = []

    def load(src, dst):
        copy = pltpu.make_async_copy(src, dst, load_sem.at[len(loads)])
        copy.start()
        loads.append(copy)

    def fid(i, j, mine=True):
        dx = other * i + core * j
        dz = core * i + other * j
        return lax.rem(zlo + dz, 4) * 4 + lax.rem(x + dx, 4)

    load(in_hbm, mixw.at[core, fs, y, 0])
    load(out_hbm, mixw.at[core, fs, y, 1])
    load(up_hbm, upw.at[core, fs])
    load(down_hbm, downw.at[fs, core])
    load(group_hbm.at[0], groupw.at[tp])
    load(scale_hbm, scales.at[tp])
    load(tokens_hbm, tok.at[pl.ds(HALO, ROWS)])

    barrier = pltpu.get_barrier_semaphore()
    for device in neighbours:
        pl.semaphore_signal(barrier, inc=1, device_id=device, device_id_type=MESH)
    pl.semaphore_wait(barrier, len(neighbours))
    for copy in loads:
        copy.wait()

    sent = []

    def message(src, dst, k, device):
        return pltpu.make_async_remote_copy(
            src_ref=src, dst_ref=dst, send_sem=send_sem.at[k], recv_sem=recv_sem.at[k],
            device_id=device, device_id_type=MESH,
        )

    def send(ref, k, device, dst=None):
        copy = message(ref, ref if dst is None else dst, k, device)
        copy.start()
        sent.append(copy)

    def arrive(ref, k):
        message(ref, ref, k, partner).wait_recv()

    def block(m, c, f, half=None):
        if m == DOWN:
            ref = downw.at[f, c]
            return ref if half is None else ref.at[pl.ds(512 * half, 512)]
        if m == UP:
            ref = upw.at[c, f]
            return ref if half is None else ref.at[pl.ds(64 * half, 64)]
        ref = mixw.at[c, f]
        return ref if half is None else ref.at[pl.ds(2 * half, 2)]

    def mine(m, i, j, half=None):
        return block(m, core, fid(i, j), half)

    def base(m, i=None):
        return m * PER_MATRIX + (0 if i is None else 4 + 4 * i)

    def relay(m, i, j):
        send(mine(m, i, j), m * PER_MATRIX + 20 + 4 * i + j, partner)

    def second(m, i):
        send(mine(m, i, 0), base(m, i), b_plus)
        send(mine(m, i, 0), base(m, i) + 1, b_minus)

    def start_own(m):
        send(mine(m, 0, 0), base(m), a_plus)
        send(mine(m, 0, 0), base(m) + 1, a_minus)
        second(m, 0)
        relay(m, 0, 0)

    def first_minus(m):
        arrive(mine(m, 3, 0), base(m))
        send(mine(m, 3, 0, 0), base(m) + 2, a_plus)
        second(m, 3)
        relay(m, 3, 0)

    def first_plus(m):
        arrive(mine(m, 1, 0), base(m) + 1)
        send(mine(m, 1, 0, 1), base(m) + 3, a_minus)
        second(m, 1)
        relay(m, 1, 0)

    def first_far(m):
        arrive(mine(m, 2, 0, 0), base(m) + 2)
        arrive(mine(m, 2, 0, 1), base(m) + 3)
        second(m, 2)
        relay(m, 2, 0)

    def turn(m, i):
        k = base(m, i)
        arrive(mine(m, i, 3), k)
        send(mine(m, i, 3, 0), k + 2, b_plus)
        relay(m, i, 3)
        arrive(mine(m, i, 1), k + 1)
        send(mine(m, i, 1, 1), k + 3, b_minus)
        relay(m, i, 1)

    def last(m, i):
        k = base(m, i)
        arrive(mine(m, i, 2, 0), k + 2)
        arrive(mine(m, i, 2, 1), k + 3)
        relay(m, i, 2)

    def swapped(m, i, j):
        arrive(block(m, other, fid(j, i)), m * PER_MATRIX + 20 + 4 * i + j)

    def swapped_all(m):
        for i in range(4):
            for j in range(4):
                swapped(m, i, j)

    own_mix = mixw.at[core, fs, y]
    for n, device in ((1, y_plus), (3, y_minus), (2, y_far)):
        send(own_mix, Y_BASE + n, device)
    next_tp = lax.rem(tp + 1, 8)
    send(tok.at[pl.ds(HALO + ROWS - HALO, HALO)], HALO_K, (rep, fs, next_tp), tok.at[pl.ds(0, HALO)])
    for n, device in ((1, y_plus), (3, y_minus), (2, y_far)):
        send(groupw.at[tp], Y_BASE + 4 + n, device)
        send(scales.at[tp], Y_BASE + 8 + n, device)
    send(groupw.at[tp], Y_BASE + 4, partner)
    send(scales.at[tp], Y_BASE + 8, partner)
    start_own(UP)

    arrive(tok.at[pl.ds(0, HALO)], HALO_K)

    def norm_rows(r, carry):
        rows = tok[pl.ds(pl.multiple_of(r * 16, 16), 16), :].astype(F32)
        scale = lax.rsqrt(jnp.mean(rows * rows, axis=-1, keepdims=True) + EPS)
        values = (rows * scale * gain1[...]).astype(BF16)
        for f in range(16):
            normed[f, pl.ds(pl.multiple_of(r * 16, 16), 16), :] = values[:, f * 128 : (f + 1) * 128]
        return carry

    lax.fori_loop(0, EXT // 16, norm_rows, 0)

    def line(n):
        return lax.rem(y + n, 4)

    for n in (1, 3, 2):
        arrive(mixw.at[core, fs, line(4 - n)], Y_BASE + n)
    start_own(MIX)
    first_minus(MIX)
    first_plus(MIX)
    turn(MIX, 0)
    first_far(MIX)
    turn(MIX, 3)
    turn(MIX, 1)
    turn(MIX, 2)
    first_minus(UP)
    first_plus(UP)
    first_far(UP)
    for n in (1, 3, 2):
        from_tp = line(4 - n) * 2 + core
        arrive(groupw.at[from_tp], Y_BASE + 4 + n)
        arrive(scales.at[from_tp], Y_BASE + 8 + n)
        send(groupw.at[from_tp], Y_BASE + 12 + n, partner)
    for n in (1, 3, 2):
        from_tp = line(4 - n) * 2 + core
        send(scales.at[from_tp], N_SEMS + n, partner)
    for i in ORDER:
        last(MIX, i)
    arrive(groupw.at[y * 2 + other], Y_BASE + 4)
    arrive(scales.at[y * 2 + other], Y_BASE + 8)
    for n in (1, 3, 2):
        from_tp = line(4 - n) * 2 + other
        arrive(groupw.at[from_tp], Y_BASE + 12 + n)
        arrive(scales.at[from_tp], N_SEMS + n)
    swapped_all(MIX)

    acc[...] = jnp.zeros_like(acc)

    def project(q, carry):
        left = jnp.concatenate([normed[2 * q], normed[2 * q + 1]], axis=1)
        right = jnp.concatenate(
            [
                jnp.concatenate([mixw[t % 2, 2 * q + s, t // 2, 0] for t in range(8)], axis=1)
                for s in range(2)
            ],
            axis=0,
        )
        acc[...] += jnp.dot(left, right, preferred_element_type=F32)
        return carry

    lax.fori_loop(0, 8, project, 0)

    row = lax.broadcasted_iota(jnp.int32, (EXT, 128), 0)
    first_of_sequence = jnp.where(tp == 0, HALO, 0)
    position = tp * ROWS + lax.broadcasted_iota(jnp.int32, (ROWS, 128), 0)
    for g in range(8):
        values = acc[:, g * 128 : (g + 1) * 128].astype(BF16).astype(F32)
        values = jnp.where(row >= first_of_sequence, values, 0.0)
        running = values
        for level in range(g % 4 + 1):
            running = running + pltpu.roll(running, 2**level, 0)
        count = jnp.minimum(position + 1, 2 ** (g % 4 + 1)).astype(F32)
        pooled = (running[HALO:] / count - values[HALO:]).astype(BF16)
        mapped = jnp.dot(pooled, groupw[g], preferred_element_type=F32)
        pool[:, g * 128 : (g + 1) * 128] = (mapped * scales[g]).astype(BF16)

    for f in range(16):
        mixed[f] = tok[HALO:, f * 128 : (f + 1) * 128].astype(F32)

    def project_out(q, squares):
        right = jnp.concatenate(
            [
                jnp.concatenate([mixw[t % 2, 2 * q + s, t // 2, 1] for t in range(8)], axis=0)
                for s in range(2)
            ],
            axis=1,
        )
        added = jnp.dot(pool[...], right, preferred_element_type=F32)
        for s in range(2):
            part = mixed[2 * q + s] + added[:, s * 128 : (s + 1) * 128]
            mixed[2 * q + s] = part
            squares = squares + part * part
        return squares

    squares = lax.fori_loop(0, 8, project_out, jnp.zeros((ROWS, 128), F32))
    scale = lax.rsqrt(jnp.sum(squares, axis=-1, keepdims=True) * (1.0 / 2048) + EPS)
    for f in range(16):
        cols = slice(f * 128, (f + 1) * 128)
        gathered[0, :, cols] = (mixed[f] * scale * gain2[:, cols]).astype(BF16)

    def rows_of(n, half):
        return gathered.at[n, pl.ds(64 * half, 64)]

    send(rows_of(0, 0), AG_BASE + 0, y_plus, rows_of(3, 0))
    send(rows_of(0, 1), AG_BASE + 1, y_minus, rows_of(1, 1))
    send(rows_of(0, 1), AG_BASE + 2, y_plus, rows_of(3, 1))
    send(rows_of(0, 0), AG_BASE + 3, y_minus, rows_of(1, 0))

    turn(UP, 0)
    turn(UP, 3)
    start_own(DOWN)
    arrive(rows_of(3, 0), AG_BASE + 0)
    send(rows_of(3, 0), AG_BASE + 4, y_plus, rows_of(2, 0))
    arrive(rows_of(1, 1), AG_BASE + 1)
    send(rows_of(1, 1), AG_BASE + 5, y_minus, rows_of(2, 1))
    turn(UP, 1)
    turn(UP, 2)
    first_minus(DOWN)
    first_plus(DOWN)
    first_far(DOWN)
    for i in ORDER:
        last(UP, i)
    swapped_all(UP)

    def up_rows(n):
        def body(t, carry):
            c = lax.div(t, 4)
            cols = pl.ds(pl.multiple_of(lax.rem(t, 4) * 256, 256), 256)
            right = upw[c, :, :, cols].reshape(2048, 256)
            value = jnp.maximum(jnp.dot(gathered[n], right, preferred_element_type=F32), 0.0)
            hidden[n, :, pl.ds(pl.multiple_of(t * 256, 256), 256)] = (value * value).astype(BF16)
            return carry

        lax.fori_loop(0, 8, body, 0)

    up_rows(0)
    turn(DOWN, 0)
    arrive(rows_of(3, 1), AG_BASE + 2)
    up_rows(3)
    turn(DOWN, 3)
    arrive(rows_of(1, 0), AG_BASE + 3)
    up_rows(1)
    turn(DOWN, 1)
    arrive(rows_of(2, 0), AG_BASE + 4)
    arrive(rows_of(2, 1), AG_BASE + 5)
    up_rows(2)
    turn(DOWN, 2)
    for i in ORDER:
        last(DOWN, i)
    swapped_all(DOWN)

    for g in range(8):
        right = jnp.concatenate([downw[2 * g + s].reshape(2048, 128) for s in range(2)], axis=1)
        part = jnp.dot(hidden[...].reshape(512, 2048), right, preferred_element_type=F32)
        far_out[g] = part[256:384].astype(BF16)
        k = RS_BASE + 4 * g
        send(far_out.at[g, pl.ds(0, 64)], k, y_plus, far_in.at[g, 0])
        send(far_out.at[g, pl.ds(64, 64)], k + 1, y_minus, far_in.at[g, 1])
        for s in range(2):
            mixed[2 * g + s] += part[0:128, s * 128 : (s + 1) * 128]
        near_out[g, 0, 64:] = part[192:256].astype(BF16)
        near_out[g, 1, :64] = part[384:448].astype(BF16)
        keep[g, 0] = part[128:192]
        keep[g, 1] = part[448:512]

    def pass_on(g):
        k = RS_BASE + 4 * g
        arrive(far_in.at[g, 0], k)
        near_out[g, 0, :64] = (keep[g, 0] + far_in[g, 0].astype(F32)).astype(BF16)
        send(near_out.at[g, 0], k + 2, y_plus, near_in.at[g, 0])
        arrive(far_in.at[g, 1], k + 1)
        near_out[g, 1, 64:] = (keep[g, 1] + far_in[g, 1].astype(F32)).astype(BF16)
        send(near_out.at[g, 1], k + 3, y_minus, near_in.at[g, 1])

    def finish(g):
        k = RS_BASE + 4 * g
        arrive(near_in.at[g, 0], k + 2)
        arrive(near_in.at[g, 1], k + 3)
        for s in range(2):
            cols = slice(s * 128, (s + 1) * 128)
            total = mixed[2 * g + s] + (
                near_in[g, 0, :, cols].astype(F32) + near_in[g, 1, :, cols].astype(F32)
            )
            o_ref[:, (2 * g + s) * 128 : (2 * g + s + 1) * 128] = total.astype(BF16)

    for g in range(8):
        pass_on(g)
    for g in range(8):
        finish(g)
    for copy in sent:
        copy.wait_send()


def local(tokens, gain1, in_w, group_w, scale, out_w, gain2, up_w, down_w):
    any_space = pl.BlockSpec(memory_space=pl.ANY)
    vmem = pl.BlockSpec(memory_space=pltpu.VMEM)
    return pl.pallas_call(
        kernel,
        out_shape=jax.ShapeDtypeStruct((ROWS, 2048), BF16),
        in_specs=[any_space, vmem, any_space, any_space, any_space, any_space, vmem, any_space, any_space],
        out_specs=vmem,
        scratch_shapes=[
            pltpu.VMEM((EXT, 2048), BF16),
            pltpu.VMEM((2, 16, 4, 2, 128, 128), BF16),
            pltpu.VMEM((2, 16, 128, 1024), BF16),
            pltpu.VMEM((16, 2, 1024, 128), BF16),
            pltpu.VMEM((8, 128, 128), BF16),
            pltpu.VMEM((8, 1, 128), F32),
            pltpu.VMEM((16, EXT, 128), BF16),
            pltpu.VMEM((EXT, 1024), F32),
            pltpu.VMEM((16, ROWS, 128), F32),
            pltpu.VMEM((ROWS, 1024), BF16),
            pltpu.VMEM((4, ROWS, 2048), BF16),
            pltpu.VMEM((4, ROWS, 2048), BF16),
            pltpu.VMEM((8, ROWS, 256), BF16),
            pltpu.VMEM((8, 2, 64, 256), BF16),
            pltpu.VMEM((8, 2, ROWS, 256), BF16),
            pltpu.VMEM((8, 2, ROWS, 256), BF16),
            pltpu.VMEM((8, 2, 64, 256), F32),
            pltpu.SemaphoreType.DMA((N_SEMS + 4,)),
            pltpu.SemaphoreType.DMA((N_SEMS + 4,)),
            pltpu.SemaphoreType.DMA((7,)),
        ],
        compiler_params=pltpu.CompilerParams(
            collective_id=0, has_side_effects=True, vmem_limit_bytes=62 * 1024 * 1024
        ),
        cost_estimate=pl.CostEstimate(flops=10_000_000_000, bytes_accessed=3_000_000, transcendentals=0),
        name="layer",
    )(tokens, gain1.reshape(1, 2048), in_w, group_w, scale.reshape(1, 128), out_w, gain2.reshape(1, 2048), up_w, down_w)


def solution(mesh):
    in_specs = (
        P(("rep", "fs", "tp"), None),
        P(),
        P("fs", "tp"),
        P("tp", None, None),
        P("tp"),
        P("tp", "fs"),
        P(),
        P("fs", "tp"),
        P("tp", "fs"),
    )
    return jax.shard_map(
        local, mesh=mesh, in_specs=in_specs, out_specs=P(("rep", "fs", "tp"), None), check_vma=False
    )
```

time: 298 us -> 113 us (0.38)
  waiting for transfers between devices: 140 us -> 0 us
  Pallas kernels: 0 us -> 111 us
  blocking collectives: 55.7 us -> 0 us
  local copies, waits for them, and re-layouts: 31.4 us -> 1.88 us
  starting transfers between devices: 23.6 us -> 0 us
  matrix products: 21.4 us -> 0 us
  between operations: 14.8 us -> 0.01 us
  other arithmetic: 10.2 us -> 0 us
    pallas_call x0 -> x1, Pallas kernels: none -> 111 us  [local(): pl.pallas_call(kernel, out_shape=jax.ShapeDtypeStruct((ROWS, 2048), BF16)...]
    all_to_all x4 -> x0, blocking collectives: 55.7 us -> none  [the longest x1 29.4 us: summed_rows(): lax.all_to_all(nearer.astype(jnp.bfloat16), far, split_axis=0, concat_axi...]
    all_to_all x4 -> x0, waiting for transfers between devices: 51.7 us -> none  [copy_for_each(): lax.all_to_all(jnp.broadcast_to(x[None], (peers, *x.shape)), axis, 0, 0,...]
    all_gather x4 -> x0, waiting for transfers between devices: 47.2 us -> none  [all_blocks(): pieces = lax.all_gather(pieces, axes[k])]
    reduce_scatter x1 -> x0, waiting for transfers between devices: 38.3 us -> none  [local(): lax.psum_scatter(jnp.dot(block_rows, out_local, preferred_element_type=jn...]
    all_to_all x4 -> x0, starting transfers between devices: 23.5 us -> none  [copy_for_each(): lax.all_to_all(jnp.broadcast_to(x[None], (peers, *x.shape)), axis, 0, 0,...]
    dot_general x3 -> x0, matrix products: 21.4 us -> none  [the longest x1 14.4 us: local(): jnp.dot(block_rows, down_local, preferred_element_type=jnp.float32)]
    transpose x3 -> x0, local copies, waits for them, and re-layouts: 15.7 us -> none  [the longest x2 9.27 us: all_blocks(): pieces = pieces.transpose(*back, *range(len(axes), pieces.ndim))]
  transfers between devices with their start and end apart: 9 -> 0, of which waited for: 6 -> 0; matrix products, arithmetic and copies ran while one was open for 12% -> 0% of each run, Pallas kernels for 0% -> 0%
where the time goes in v1:
time: 113 us
  Pallas kernels  111 us (98%)
  local copies, waits for them, and re-layouts  1.88 us (2%)
    pallas_call x1, Pallas kernels, local(): pl.pallas_call(kernel, out_shape=jax.ShapeDtypeStruct((ROWS, 2048), BF16)...  111 us

profile of v1, /device:TPU:1, one launch (start us, length us, event | category | flops | bytes accessed | tf_op | source)
XLA Modules:
  0.0 113.0 jit_solution(3440779475543745359)
XLA Ops:
  0.0 111.1 %layer.1 = bf16[128,2048]{1,0:T(8,128)(2,1)} custom-call(bf16[128,2048]{1,0:T(8,128)(2,1)} %tokens_hbm.1, f32[1,2048]{1,0:T(1,128)} %bitcast.3, bf16[128,128]{1,0:T(8,128)(2,1)} %in_hbm.1, bf16[1,128,128]{2,1,0:T(8,128)(2,1)} %group_hbm.1, f32[1,128]{1,0:T(1,128)} %bitcast.5, bf16[128,128]{1,0:T(8,128)(2,1)} %out_hbm.1, f32[1,2048]{1,0:T(1,128)} %bitcast.4, ...), custom_call_target="tpu_custom_call" | custom-call | flops 10000000000 | bytes 3000000 | tf_op jit(solution)/shard_map/layer/pallas_call | solution.py:388
  111.1 1.9 %copy.11 = bf16[128,2048]{1,0:T(8,128)(2,1)} copy(bf16[128,2048]{1,0:T(8,128)(2,1)} %layer.1) | data formatting | bytes 1048576

commit v2 on v1

v2 whole, which is shorter than its diff:
```python
import jax
import jax.numpy as jnp
from jax import lax
from jax.experimental import pallas as pl
from jax.experimental.pallas import tpu as pltpu
from jax.sharding import PartitionSpec as P

EPS = 1e-06
MESH = pl.DeviceIdType.MESH
F32 = jnp.float32
BF16 = jnp.bfloat16
HALO = 16
ROWS = 128
EXT = HALO + ROWS
HEAD = 96
TAIL = 128 - HEAD
ORDER = (0, 3, 1, 2)
OUT, UP, DOWN = "out", "up", "down"
OWN, PLUS, MINUS, FAR = 0, 1, 2, 3
N_SEMS = 128
N_KINDS = 16


def kernel(
    tokens_hbm, gain1, in_hbm, group_hbm, scale_hbm, out_hbm, gain2, up_hbm, down_hbm,
    o_ref,
    tok, inw, outw, upw, downw, groupw, scales,
    normed_heads, normed_tails, acc, mixed, pool, gathered, hidden,
    far_out, far_in, near_out, near_in, keep,
    send_sem, recv_sem, load_sem,
):
    rep = lax.axis_index("rep")
    fs = lax.axis_index("fs")
    tp = lax.axis_index("tp")
    x = lax.rem(fs, 4)
    zlo = lax.div(fs, 4)
    z = rep * 4 + zlo
    y = lax.div(tp, 2)
    core = lax.rem(tp, 2)
    other = 1 - core
    a = other * x + core * zlo
    b = core * x + other * zlo

    def at(x_, z_, tp_):
        return (lax.div(z_, 4), lax.rem(z_, 4) * 4 + x_, tp_)

    def step(first_axis, d):
        on_x = other if first_axis else core
        on_z = core if first_axis else other
        return at(lax.rem(x + on_x * d + 4, 4), lax.rem(z + on_z * d + 8, 8), tp)

    a_plus, a_minus = step(True, 1), step(True, -1)
    b_plus, b_minus = step(False, 1), step(False, -1)
    partner = (rep, fs, y * 2 + other)

    def on_y(d, c):
        return (rep, fs, lax.rem(y + d + 4, 4) * 2 + c)

    y_plus, y_minus, y_far = on_y(1, core), on_y(-1, core), on_y(2, core)
    neighbours = (
        a_plus, a_minus, b_plus, b_minus, partner, y_plus, y_minus, y_far,
        on_y(1, other), on_y(-1, other),
    )
    barrier = pltpu.get_barrier_semaphore()
    for device in neighbours:
        pl.semaphore_signal(barrier, inc=1, device_id=device, device_id_type=MESH)

    def line(n):
        return lax.rem(y + n, 4)

    def fid(i, j):
        dx = other * i + core * j
        dz = core * i + other * j
        return lax.rem(zlo + dz, 4) * 4 + lax.rem(x + dx, 4)

    loads = []

    def load(src, dst):
        copy = pltpu.make_async_copy(src, dst, load_sem.at[len(loads)])
        copy.start()
        loads.append(copy)

    load(tokens_hbm, tok.at[pl.ds(HALO, ROWS)])
    load(in_hbm.at[pl.ds(0, HEAD)], inw.at[core, y, a * 4 + b])
    load(in_hbm.at[pl.ds(HEAD, TAIL)], outw.at[core, fs, y, pl.ds(128, TAIL)])
    load(out_hbm, outw.at[core, fs, y, pl.ds(0, 128)])
    load(up_hbm, upw.at[core, fs])
    load(down_hbm, downw.at[fs, core])
    load(group_hbm.at[0], groupw.at[tp])
    load(scale_hbm, scales.at[tp])

    def norm_rows(r, carry):
        at_rows = pl.ds(pl.multiple_of(r * 16, 16), 16)
        rows = tok[at_rows, :].astype(F32)
        scale = lax.rsqrt(jnp.mean(rows * rows, axis=-1, keepdims=True) + EPS)
        values = rows * scale * gain1[...]
        heads = [values[:, f * 128 : f * 128 + HEAD] for f in range(16)]
        tails = [values[:, f * 128 + HEAD : (f + 1) * 128] for f in range(16)]
        normed_heads[at_rows, :] = jnp.concatenate(heads, axis=1).astype(BF16)
        normed_tails[at_rows, :] = jnp.concatenate(tails, axis=1).astype(BF16)
        return carry

    loads[0].wait()
    lax.fori_loop(1, EXT // 16, norm_rows, 0)
    for f in range(16):
        mixed[f] = tok[HALO:, f * 128 : (f + 1) * 128].astype(F32)
    for copy in loads[1:]:
        copy.wait()
    pl.semaphore_wait(barrier, len(neighbours))

    numbers = {}
    used = [0]

    def number(*name, count=1):
        if name not in numbers:
            numbers[name] = used[0]
            used[0] += count
            assert used[0] <= N_SEMS, used
        return numbers[name]

    kinds = {}

    def message(src, dst, k, kind, device):
        return pltpu.make_async_remote_copy(
            src_ref=src, dst_ref=dst, send_sem=send_sem.at[kinds.setdefault(kind, len(kinds))],
            recv_sem=recv_sem.at[k], device_id=device, device_id_type=MESH,
        )

    def send(kind, ref, k, device, dst=None):
        message(ref, ref if dst is None else dst, k, kind, device).start()

    def arrive(ref, k):
        message(ref, ref, k, "halo", partner).wait_recv()

    def all_sent(kind, ref):
        message(ref, ref, 0, kind, partner).wait_send()

    def block(m, c, f, half=None):
        if m == DOWN:
            ref = downw.at[f, c]
            return ref if half is None else ref.at[pl.ds(512 * half, 512)]
        if m == UP:
            ref = upw.at[c, f]
            return ref if half is None else ref.at[pl.ds(64 * half, 64)]
        ref = outw.at[c, f]
        return ref if half is None else ref.at[pl.ds(2 * half, 2)]

    def mine(m, i, j, half=None):
        return block(m, core, fid(i, j), half)

    def done(m, i, j):
        k = number(m, "relay", count=4 if m == DOWN else 1)
        if m == DOWN:
            k = k + core * i + other * j
        send((m, "relay"), mine(m, i, j), k, partner)

    def second(m, i):
        send(m, mine(m, i, 0), number(m, i, 3), b_plus)
        send(m, mine(m, i, 0), number(m, i, 1), b_minus)

    def begin(m):
        if m == OUT:
            arrive(outw.at[core, fs, line(2)], number("outy", 2))
        send(m, mine(m, 0, 0), number(m, 3), a_plus)
        send(m, mine(m, 0, 0), number(m, 1), a_minus)
        second(m, 0)
        done(m, 0, 0)

    def first(m, i):
        arrive(mine(m, i, 0), number(m, i))
        half = 0 if i == 3 else 1
        send(m, mine(m, i, 0, half), number(m, 2), a_plus if i == 3 else a_minus)
        second(m, i)
        done(m, i, 0)

    def first_far(m):
        arrive(mine(m, 2, 0), number(m, 2))
        second(m, 2)
        done(m, 2, 0)

    def turn(m, i, j):
        arrive(mine(m, i, j), number(m, i, j))
        half = 0 if j == 3 else 1
        send(m, mine(m, i, j, half), number(m, i, 2), b_plus if j == 3 else b_minus)
        done(m, i, j)

    def last(m, i):
        arrive(mine(m, i, 2), number(m, i, 2))
        done(m, i, 2)

    def swapped(m):
        arrive(outw.at[other] if m == OUT else upw.at[other], number(m, "relay"))

    def swapped_row(m, r):
        arrive(downw.at[pl.ds(lax.rem(zlo + r, 4) * 4, 4), other], number(m, "relay", count=4) + r)

    def inblock(n, i, j, half=None):
        ref = inw.at[core, line(n), lax.rem(a + i, 4) * 4 + lax.rem(b + j, 4)]
        return ref if half is None else ref.at[pl.ds(HEAD // 2 * half, HEAD // 2)]

    def ingroup(n, i, half=None):
        start = lax.rem(a + i, 4) * 4
        if half is None:
            return inw.at[core, line(n), pl.ds(start, 4)]
        return inw.at[core, line(n), pl.ds(start + 2 * half, 2)]

    def in_relay(n, i):
        send("inrelay", ingroup(n, i), number("inrelay", n), partner)

    def in_swapped(n):
        arrive(inw.at[other, line(n)], number("inrelay", n))

    def y_send(j):
        send("iny", inblock(0, 0, j), number("iny", 3, 0, j), y_plus)
        send("iny", inblock(0, 0, j), number("iny", 1, 0, j), y_minus)

    def y_turn(i, j):
        arrive(inblock(3, i, j), number("iny", 3, i, j))
        arrive(inblock(1, i, j), number("iny", 1, i, j))
        send("iny", inblock(3, i, j, 0), number("iny", 2, i), y_plus)
        send("iny", inblock(1, i, j, 1), number("iny", 2, i), y_minus)

    def y_group(i):
        arrive(ingroup(3, i), number("iny", 3, i))
        arrive(ingroup(1, i), number("iny", 1, i))
        send("iny", ingroup(3, i, 0), number("iny", 2, i), y_plus)
        send("iny", ingroup(1, i, 1), number("iny", 2, i), y_minus)
        y_relay(i)

    def y_relay(i=0):
        in_relay(3, i)
        in_relay(1, i)

    def y_last(i):
        arrive(ingroup(2, i), number("iny", 2, i))
        in_relay(2, i)

    def in_second(i):
        send("in", inblock(0, i, 0), number("in", i, 3), b_plus)
        send("in", inblock(0, i, 0), number("in", i, 1), b_minus)

    def in_first(i):
        arrive(inblock(0, i, 0), number("in", i))
        half = 0 if i == 3 else 1
        send("in", inblock(0, i, 0, half), number("in", 2), a_plus if i == 3 else a_minus)
        in_second(i)

    def in_first_far():
        arrive(inblock(0, 2, 0), number("in", 2))
        in_second(2)

    def in_turn(i, j):
        arrive(inblock(0, i, j), number("in", i, j))
        half = 0 if j == 3 else 1
        send("in", inblock(0, i, j, half), number("in", i, 2), b_plus if j == 3 else b_minus)
        if i == 0:
            y_send(j)

    def in_last(i):
        arrive(inblock(0, i, 2), number("in", i, 2))
        if i == 0:
            y_send(2)
        else:
            send("iny", ingroup(0, i), number("iny", 3, i), y_plus)
            send("iny", ingroup(0, i), number("iny", 1, i), y_minus)
        in_relay(0, i)

    def outy(n, half=None):
        ref = outw.at[core, fs, line(n)]
        return ref if half is None else ref.at[pl.ds((128 + TAIL) // 2 * half, (128 + TAIL) // 2)]

    def groupy(n, half=None, c=core):
        ref = groupw.at[line(n) * 2 + c]
        return ref if half is None else ref.at[pl.ds(64 * half, 64)]

    def scaley(n, c=core):
        return scales.at[line(n) * 2 + c]

    def pass_out():
        arrive(outy(3), number("outy", 3))
        arrive(outy(1), number("outy", 1))
        send("outy", outy(3, 0), number("outy", 2), y_plus)
        send("outy", outy(1, 1), number("outy", 2), y_minus)

    def group_relay(n):
        send("group", groupy(n), number("grouprelay", n), partner)
        send("scale", scaley(n), number("scalerelay", n), partner)

    def pass_group():
        for n in (3, 1):
            arrive(groupy(n), number("group", n))
            arrive(scaley(n), number("scale", n))
        send("group", groupy(3, 0), number("group", 2), y_plus)
        send("group", groupy(1, 1), number("group", 2), y_minus)
        group_relay(3)
        group_relay(1)

    def small_ones():
        arrive(tok.at[pl.ds(0, HALO)], number("halo"))
        norm_rows(0, 0)
        arrive(groupy(2), number("group", 2))
        arrive(scaley(2), number("scale", 2))
        group_relay(2)

    def small_swapped():
        for n in ORDER:
            arrive(groupy(n, c=other), number("grouprelay", n))
            arrive(scaley(n, c=other), number("scalerelay", n))

    send("outy", outy(0), number("outy", 3), y_plus)
    send("outy", outy(0), number("outy", 1), y_minus)
    send("in", inblock(0, 0, 0), number("in", 3), a_plus)
    send("in", inblock(0, 0, 0), number("in", 1), a_minus)
    in_second(0)
    y_send(0)
    send("group", groupy(0), number("group", 3), y_plus)
    send("group", groupy(0), number("group", 1), y_minus)
    for n, device in ((3, y_plus), (1, y_minus), (2, y_far)):
        send("scale", scaley(0), number("scale", n), device)
    group_relay(0)
    send(
        "halo", tok.at[pl.ds(ROWS, HALO)], number("halo"), (rep, fs, lax.rem(tp + 1, 8)),
        tok.at[pl.ds(0, HALO)],
    )

    row = lax.broadcasted_iota(jnp.int32, (EXT, 128), 0)
    first_of_sequence = jnp.where(tp == 0, HALO, 0)
    position = tp * ROWS + lax.broadcasted_iota(jnp.int32, (ROWS, 128), 0)

    def project(n):
        in_swapped(n)
        q = line(n)
        right = jnp.concatenate(
            [
                jnp.concatenate([inw[0, q, (f % 4) * 4 + f // 4], inw[1, q, f]], axis=1)
                for f in range(16)
            ],
            axis=0,
        )
        acc[n] = jnp.dot(normed_heads[...], right, preferred_element_type=F32)

    def project_out(n):
        q = line(n)
        right = jnp.concatenate(
            [
                jnp.concatenate([outw[c, f, q, 128 : 128 + TAIL] for c in range(2)], axis=1)
                for f in range(16)
            ],
            axis=0,
        )
        acc[n] += jnp.dot(normed_tails[...], right, preferred_element_type=F32)
        for c in range(2):
            g = 2 * q + c
            level = lax.rem(g, 4)
            values = acc[n, :, c * 128 : (c + 1) * 128].astype(BF16).astype(F32)
            values = jnp.where(row >= first_of_sequence, values, 0.0)
            running = values + pltpu.roll(values, 1, 0)
            width = 2
            for step_level in range(1, 4):
                wider = running + pltpu.roll(running, 2**step_level, 0)
                running = jnp.where(level >= step_level, wider, running)
                width = jnp.where(level >= step_level, 2 ** (step_level + 1), width)
            count = jnp.minimum(position + 1, width).astype(F32)
            pooled = (running[HALO:] / count - values[HALO:]).astype(BF16)
            mapped = jnp.dot(pooled, groupw[g], preferred_element_type=F32)
            pool[n, :, c * 128 : (c + 1) * 128] = (mapped * scales[g]).astype(BF16)
        for p in range(8):
            right = jnp.concatenate(
                [
                    jnp.concatenate([outw[c, 2 * p + s, q, 0:128] for c in range(2)], axis=0)
                    for s in range(2)
                ],
                axis=1,
            )
            added = jnp.dot(pool[n], right, preferred_element_type=F32)
            for s in range(2):
                mixed[2 * p + s] += added[:, s * 128 : (s + 1) * 128]

    def rows_of(slot, half):
        return gathered.at[slot, pl.ds(64 * half, 64)]

    def norm_two():
        squares = mixed[0] * mixed[0]
        for f in range(1, 16):
            squares = squares + mixed[f] * mixed[f]
        scale = lax.rsqrt(jnp.sum(squares, axis=-1, keepdims=True) * (1.0 / 2048) + EPS)
        for f in range(16):
            cols = slice(f * 128, (f + 1) * 128)
            gathered[OWN, :, cols] = (mixed[f] * scale * gain2[:, cols]).astype(BF16)
        for half, device, slot in (
            (0, y_plus, MINUS), (1, y_minus, PLUS), (1, y_plus, MINUS), (0, y_minus, PLUS),
        ):
            send("ag", rows_of(OWN, half), number("ag", slot, half), device, rows_of(slot, half))

    def to_far_plus():
        arrive(rows_of(MINUS, 0), number("ag", MINUS, 0))
        send("ag", rows_of(MINUS, 0), number("ag", FAR), y_plus, rows_of(FAR, 0))

    def to_far_minus():
        arrive(rows_of(PLUS, 1), number("ag", PLUS, 1))
        send("ag", rows_of(PLUS, 1), number("ag", FAR), y_minus, rows_of(FAR, 1))

    def rows_near():
        arrive(rows_of(MINUS, 1), number("ag", MINUS, 1))
        arrive(rows_of(PLUS, 0), number("ag", PLUS, 0))

    def rows_far():
        arrive(gathered.at[FAR], number("ag", FAR))

    def up_rows(start, slots):
        left = gathered[start : start + slots].reshape(slots * ROWS, 2048)

        def body(c, carry):
            right = upw[c].reshape(2048, 1024)
            value = jnp.maximum(jnp.dot(left, right, preferred_element_type=F32), 0.0)
            value = (value * value).astype(BF16).reshape(slots, ROWS, 1024)
            hidden[start : start + slots, :, pl.ds(pl.multiple_of(c * 1024, 1024), 1024)] = value
            return carry

        lax.fori_loop(0, 2, body, 0)

    def up_own():
        up_rows(OWN, 1)

    def up_near():
        up_rows(PLUS, 2)

    def up_far():
        up_rows(FAR, 1)

    def columns(g, s):
        return lax.rem(zlo + ORDER[g // 2], 4) * 4 + (g % 2) * 2 + s

    def down(g, slot):
        right = jnp.concatenate([downw[columns(g, s)].reshape(2048, 128) for s in range(2)], axis=1)
        return jnp.dot(hidden[slot], right, preferred_element_type=F32)

    def down_near(g):
        part = down(g, PLUS)
        near_out[g, 0, 64:] = part[64:].astype(BF16)
        keep[g, 0] = part[:64]
        part = down(g, MINUS)
        near_out[g, 1, :64] = part[:64].astype(BF16)
        keep[g, 1] = part[64:]
        part = down(g, OWN)
        for s in range(2):
            mixed[columns(g, s)] += part[:, s * 128 : (s + 1) * 128]
        send_near(g, 0, 1, y_plus)
        send_near(g, 1, 0, y_minus)

    def send_near(g, way, half, device):
        rows = pl.ds(64 * half, 64)
        send("near", near_out.at[g, way, rows], number("near", g), device, near_in.at[g, way, rows])

    def down_far(g):
        far_out[g] = down(g, FAR).astype(BF16)
        send("far", far_out.at[g, pl.ds(0, 64)], number("far", g), y_plus, far_in.at[g, pl.ds(0, 64)])
        send("far", far_out.at[g, pl.ds(64, 64)], number("far", g), y_minus, far_in.at[g, pl.ds(64, 64)])

    def pass_on(g):
        arrive(far_in.at[g], number("far", g))
        near_out[g, 0, :64] = (keep[g, 0] + far_in[g, :64].astype(F32)).astype(BF16)
        near_out[g, 1, 64:] = (keep[g, 1] + far_in[g, 64:].astype(F32)).astype(BF16)
        send_near(g, 0, 0, y_plus)
        send_near(g, 1, 1, y_minus)

    def finish(g):
        arrive(near_in.at[g], number("near", g))
        for s in range(2):
            cols = slice(s * 128, (s + 1) * 128)
            total = mixed[columns(g, s)] + (
                near_in[g, 0, :, cols].astype(F32) + near_in[g, 1, :, cols].astype(F32)
            )
            o_ref[:, pl.ds(pl.multiple_of(columns(g, s) * 128, 128), 128)] = total.astype(BF16)

    steps = (
        (begin, UP), (in_first, 1), (in_first, 3), (pass_out,), (begin, OUT), (in_turn, 0, 3), (pass_group,),
        (in_turn, 0, 1), (in_turn, 1, 1), (in_first_far,), (in_turn, 1, 3), (in_turn, 3, 3), (in_turn, 3, 1),
        (turn, UP, 0, 1), (turn, UP, 0, 3), (first, OUT, 1), (in_last, 0), (in_turn, 2, 3), (in_last, 1),
        (in_last, 3), (first, OUT, 3), (in_turn, 2, 1), (first_far, OUT), (y_group, 1), (turn, OUT, 0, 3),
        (turn, OUT, 1, 3), (y_turn, 0, 3), (turn, OUT, 0, 1), (small_ones,), (turn, OUT, 1, 1), (y_turn, 0, 1),
        (in_last, 2), (last, UP, 0), (y_turn, 0, 0), (turn, OUT, 3, 1), (y_turn, 0, 2), (project, 0), (y_relay,),
        (turn, OUT, 3, 3), (small_swapped,), (turn, OUT, 2, 3), (turn, OUT, 2, 1), (last, OUT, 0), (first, UP, 1),
        (first, UP, 3), (y_group, 2), (y_group, 3), (y_last, 1), (last, OUT, 3), (y_last, 0), (project, 1),
        (last, OUT, 1), (begin, DOWN), (last, OUT, 2), (y_last, 2), (swapped, OUT), (project_out, 1), (y_last, 3),
        (project, 3), (project_out, 3), (project, 2), (project_out, 2), (first_far, UP), (project_out, 0),
        (norm_two,), (turn, UP, 3, 1), (turn, UP, 1, 1), (turn, UP, 3, 3), (turn, UP, 1, 3), (turn, UP, 2, 1),
        (turn, UP, 2, 3), (turn, DOWN, 0, 3), (turn, DOWN, 0, 1), (last, UP, 3), (to_far_plus,), (first, DOWN, 1),
        (to_far_minus,), (first, DOWN, 3), (last, UP, 1), (last, UP, 2), (rows_near,), (swapped, UP), (up_near,),
        (rows_far,), (first_far, DOWN), (last, DOWN, 0), (up_far,), (swapped_row, DOWN, 0), (turn, DOWN, 1, 3),
        (turn, DOWN, 1, 1), (down_far, 1), (down_far, 0), (up_own,), (down_near, 1), (turn, DOWN, 3, 1),
        (down_near, 0), (pass_on, 0), (pass_on, 1), (turn, DOWN, 3, 3), (turn, DOWN, 2, 1), (turn, DOWN, 2, 3),
        (last, DOWN, 1), (swapped_row, DOWN, 1), (down_far, 4), (down_far, 5), (down_near, 5), (finish, 1),
        (last, DOWN, 3), (swapped_row, DOWN, 3), (down_far, 2), (down_near, 4), (last, DOWN, 2), (pass_on, 4),
        (down_far, 3), (pass_on, 5), (swapped_row, DOWN, 2), (down_near, 6), (down_near, 3), (pass_on, 3),
        (down_far, 6), (down_far, 7), (finish, 3), (finish, 5), (finish, 0), (down_near, 2), (finish, 4),
        (pass_on, 6), (down_near, 7), (pass_on, 7), (pass_on, 2), (finish, 6), (finish, 7), (finish, 2),
    )
    for action, *args in steps:
        action(*args)

    for m in (UP, DOWN):
        all_sent(m, upw.at[0, pl.ds(0, 15)])
        all_sent((m, "relay"), upw.at[0])
    all_sent(OUT, outw.at[0, pl.ds(0, 15)])
    all_sent((OUT, "relay"), outw.at[0])
    all_sent("in", inw.at[0, 0, pl.ds(0, 15)])
    all_sent("iny", inw.at[0, pl.ds(0, 3)])
    all_sent("inrelay", inw.at[0])
    all_sent("outy", outw.at[0, 0, pl.ds(0, 3)])
    all_sent("halo", tok.at[pl.ds(0, HALO)])
    all_sent("group", groupw.at[pl.ds(0, 7)])
    all_sent("scale", scales.at[pl.ds(0, 7)])
    all_sent("ag", gathered.at[pl.ds(0, 3)])
    all_sent("far", far_out)
    all_sent("near", near_out)


def local(tokens, gain1, in_w, group_w, scale, out_w, gain2, up_w, down_w):
    any_space = pl.BlockSpec(memory_space=pl.ANY)
    vmem = pl.BlockSpec(memory_space=pltpu.VMEM)
    return pl.pallas_call(
        kernel,
        out_shape=jax.ShapeDtypeStruct((ROWS, 2048), BF16),
        in_specs=[any_space, vmem, any_space, any_space, any_space, any_space, vmem, any_space, any_space],
        out_specs=vmem,
        scratch_shapes=[
            pltpu.VMEM((EXT, 2048), BF16),
            pltpu.VMEM((2, 4, 16, HEAD, 128), BF16),
            pltpu.VMEM((2, 16, 4, 128 + TAIL, 128), BF16),
            pltpu.VMEM((2, 16, 128, 1024), BF16),
            pltpu.VMEM((16, 2, 1024, 128), BF16),
            pltpu.VMEM((8, 128, 128), BF16),
            pltpu.VMEM((8, 1, 128), F32),
            pltpu.VMEM((EXT, 16 * HEAD), BF16),
            pltpu.VMEM((EXT, 16 * TAIL), BF16),
            pltpu.VMEM((4, EXT, 256), F32),
            pltpu.VMEM((16, ROWS, 128), F32),
            pltpu.VMEM((4, ROWS, 256), BF16),
            pltpu.VMEM((4, ROWS, 2048), BF16),
            pltpu.VMEM((4, ROWS, 2048), BF16),
            pltpu.VMEM((8, ROWS, 256), BF16),
            pltpu.VMEM((8, ROWS, 256), BF16),
            pltpu.VMEM((8, 2, ROWS, 256), BF16),
            pltpu.VMEM((8, 2, ROWS, 256), BF16),
            pltpu.VMEM((8, 2, 64, 256), F32),
            pltpu.SemaphoreType.DMA((N_KINDS,)),
            pltpu.SemaphoreType.DMA((N_SEMS,)),
            pltpu.SemaphoreType.DMA((8,)),
        ],
        compiler_params=pltpu.CompilerParams(
            collective_id=0, has_side_effects=True, vmem_limit_bytes=62 * 1024 * 1024
        ),
        cost_estimate=pl.CostEstimate(flops=10_000_000_000, bytes_accessed=3_000_000, transcendentals=0),
        name="layer",
    )(tokens, gain1.reshape(1, 2048), in_w, group_w, scale.reshape(1, 128), out_w, gain2.reshape(1, 2048), up_w, down_w)


def solution(mesh):
    in_specs = (
        P(("rep", "fs", "tp"), None),
        P(),
        P("fs", "tp"),
        P("tp", None, None),
        P("tp"),
        P("tp", "fs"),
        P(),
        P("fs", "tp"),
        P("tp", "fs"),
    )
    return jax.shard_map(
        local, mesh=mesh, in_specs=in_specs, out_specs=P(("rep", "fs", "tp"), None), check_vma=False
    )
```

time: 113 us -> 91.6 us (0.81)
  Pallas kernels: 111 us -> 89.2 us
    pallas_call x1, Pallas kernels: 111 us -> 89.2 us  [local(): pl.pallas_call(kernel, out_shape=jax.ShapeDtypeStruct((ROWS, 2048), BF16)...]
where the time goes in v2:
time: 91.6 us; the launch traced here: 91.1 us
  Pallas kernels  89.2 us (97%)
  local copies, waits for them, and re-layouts  1.88 us (2%)
    pallas_call x1, Pallas kernels, local(): pl.pallas_call(kernel, out_shape=jax.ShapeDtypeStruct((ROWS, 2048), BF16)...  89.2 us
    unnamed x1, local copies, waits for them, and re-layouts  1.88 us

profile of v2, /device:TPU:1, one launch (start us, length us, event | category | flops | bytes accessed | tf_op | source)
XLA Modules:
  0.0 91.1 jit_solution(9233637192329676416)
XLA Ops:
  0.0 89.2 %layer.1 = bf16[128,2048]{1,0:T(8,128)(2,1)} custom-call(bf16[128,2048]{1,0:T(8,128)(2,1)} %tokens_hbm.1, f32[1,2048]{1,0:T(1,128)} %bitcast.3, bf16[128,128]{1,0:T(8,128)(2,1)} %in_hbm.1, bf16[1,128,128]{2,1,0:T(8,128)(2,1)} %group_hbm.1, f32[1,128]{1,0:T(1,128)} %bitcast.5, bf16[128,128]{1,0:T(8,128)(2,1)} %out_hbm.1, f32[1,2048]{1,0:T(1,128)} %bitcast.4, ...), custom_call_target="tpu_custom_call" | custom-call | flops 10000000000 | bytes 3000000 | tf_op jit(solution)/shard_map/layer/pallas_call | solution.py:522
  89.2 1.9 %copy.11 = bf16[128,2048]{1,0:T(8,128)(2,1)} copy(bf16[128,2048]{1,0:T(8,128)(2,1)} %layer.1) | data formatting | bytes 1048576

commit v3 on v2

--- a/solution.py
+++ b/solution.py
@@ -517,12 +517,12 @@
 
 
 def local(tokens, gain1, in_w, group_w, scale, out_w, gain2, up_w, down_w):
-    any_space = pl.BlockSpec(memory_space=pl.ANY)
+    hbm = pl.BlockSpec(memory_space=pltpu.HBM)
     vmem = pl.BlockSpec(memory_space=pltpu.VMEM)
     return pl.pallas_call(
         kernel,
-        out_shape=jax.ShapeDtypeStruct((ROWS, 2048), BF16),
-        in_specs=[any_space, vmem, any_space, any_space, any_space, any_space, vmem, any_space, any_space],
+        out_shape=pltpu.VMEM((ROWS, 2048), BF16),
+        in_specs=[hbm, vmem, hbm, hbm, hbm, hbm, vmem, hbm, hbm],
         out_specs=vmem,
         scratch_shapes=[
             pltpu.VMEM((EXT, 2048), BF16),
@@ -549,7 +549,7 @@
             pltpu.SemaphoreType.DMA((8,)),
         ],
         compiler_params=pltpu.CompilerParams(
-            collective_id=0, has_side_effects=True, vmem_limit_bytes=62 * 1024 * 1024
+            collective_id=0, has_side_effects=True, vmem_limit_bytes=56 * 1024 * 1024
         ),
         cost_estimate=pl.CostEstimate(flops=10_000_000_000, bytes_accessed=3_000_000, transcendentals=0),
         name="layer",

time: 91.6 us -> 89.7 us (0.979)
  local copies, waits for them, and re-layouts: 1.88 us -> 0.8 us
    unnamed x1, local copies, waits for them, and re-layouts: 1.88 us -> 0.8 us
where the time goes in v3:
time: 89.7 us; the launch traced here: 89.2 us
  Pallas kernels  88.4 us (99%)
    pallas_call x1, Pallas kernels, local(): pl.pallas_call(kernel, out_shape=pltpu.VMEM((ROWS, 2048), BF16), in_specs...  88.4 us

profile of v3, /device:TPU:1, one launch (start us, length us, event | category | flops | bytes accessed | tf_op | source)
XLA Modules:
  0.0 89.2 jit_solution(7914059286560903317)
XLA Ops:
  0.0 88.4 %layer.1 = bf16[128,2048]{1,0:T(8,128)(2,1)S(1)} custom-call(bf16[128,2048]{1,0:T(8,128)(2,1)} %tokens_hbm.1, f32[1,2048]{1,0:T(1,128)} %bitcast.3, bf16[128,128]{1,0:T(8,128)(2,1)} %in_hbm.1, bf16[1,128,128]{2,1,0:T(8,128)(2,1)} %group_hbm.1, f32[1,128]{1,0:T(1,128)} %bitcast.5, bf16[128,128]{1,0:T(8,128)(2,1)} %out_hbm.1, f32[1,2048]{1,0:T(1,128)} %bitcast.4, ...), custom_call_target="tpu_custom_call" | custom-call | flops 10000000000 | bytes 3000000 | tf_op jit(solution)/shard_map/layer/pallas_call | solution.py:522
  88.4 0.8 copy.11

commit v4 on v3

--- a/solution.py
+++ b/solution.py
@@ -12,8 +12,6 @@
 HALO = 16
 ROWS = 128
 EXT = HALO + ROWS
-HEAD = 96
-TAIL = 128 - HEAD
 ORDER = (0, 3, 1, 2)
 OUT, UP, DOWN = "out", "up", "down"
 OWN, PLUS, MINUS, FAR = 0, 1, 2, 3
@@ -25,7 +23,7 @@
     tokens_hbm, gain1, in_hbm, group_hbm, scale_hbm, out_hbm, gain2, up_hbm, down_hbm,
     o_ref,
     tok, inw, outw, upw, downw, groupw, scales,
-    normed_heads, normed_tails, acc, mixed, pool, gathered, hidden,
+    normed, acc, mixed, pool, gathered, hidden,
     far_out, far_in, near_out, near_in, keep,
     send_sem, recv_sem, load_sem,
 ):
@@ -81,9 +79,8 @@
         loads.append(copy)
 
     load(tokens_hbm, tok.at[pl.ds(HALO, ROWS)])
-    load(in_hbm.at[pl.ds(0, HEAD)], inw.at[core, y, a * 4 + b])
-    load(in_hbm.at[pl.ds(HEAD, TAIL)], outw.at[core, fs, y, pl.ds(128, TAIL)])
-    load(out_hbm, outw.at[core, fs, y, pl.ds(0, 128)])
+    load(in_hbm, inw.at[core, y, a * 4 + b])
+    load(out_hbm, outw.at[core, fs, y])
     load(up_hbm, upw.at[core, fs])
     load(down_hbm, downw.at[fs, core])
     load(group_hbm.at[0], groupw.at[tp])
@@ -93,11 +90,7 @@
         at_rows = pl.ds(pl.multiple_of(r * 16, 16), 16)
         rows = tok[at_rows, :].astype(F32)
         scale = lax.rsqrt(jnp.mean(rows * rows, axis=-1, keepdims=True) + EPS)
-        values = rows * scale * gain1[...]
-        heads = [values[:, f * 128 : f * 128 + HEAD] for f in range(16)]
-        tails = [values[:, f * 128 + HEAD : (f + 1) * 128] for f in range(16)]
-        normed_heads[at_rows, :] = jnp.concatenate(heads, axis=1).astype(BF16)
-        normed_tails[at_rows, :] = jnp.concatenate(tails, axis=1).astype(BF16)
+        normed[at_rows, :] = (rows * scale * gain1[...]).astype(BF16)
         return carry
 
     loads[0].wait()
@@ -196,7 +189,7 @@
 
     def inblock(n, i, j, half=None):
         ref = inw.at[core, line(n), lax.rem(a + i, 4) * 4 + lax.rem(b + j, 4)]
-        return ref if half is None else ref.at[pl.ds(HEAD // 2 * half, HEAD // 2)]
+        return ref if half is None else ref.at[pl.ds(64 * half, 64)]
 
     def ingroup(n, i, half=None):
         start = lax.rem(a + i, 4) * 4
@@ -267,7 +260,7 @@
 
     def outy(n, half=None):
         ref = outw.at[core, fs, line(n)]
-        return ref if half is None else ref.at[pl.ds((128 + TAIL) // 2 * half, (128 + TAIL) // 2)]
+        return ref if half is None else ref.at[pl.ds(64 * half, 64)]
 
     def groupy(n, half=None, c=core):
         ref = groupw.at[line(n) * 2 + c]
@@ -337,18 +330,10 @@
             ],
             axis=0,
         )
-        acc[n] = jnp.dot(normed_heads[...], right, preferred_element_type=F32)
+        acc[n] = jnp.dot(normed[...], right, preferred_element_type=F32)
 
     def project_out(n):
         q = line(n)
-        right = jnp.concatenate(
-            [
-                jnp.concatenate([outw[c, f, q, 128 : 128 + TAIL] for c in range(2)], axis=1)
-                for f in range(16)
-            ],
-            axis=0,
-        )
-        acc[n] += jnp.dot(normed_tails[...], right, preferred_element_type=F32)
         for c in range(2):
             g = 2 * q + c
             level = lax.rem(g, 4)
@@ -367,7 +352,7 @@
         for p in range(8):
             right = jnp.concatenate(
                 [
-                    jnp.concatenate([outw[c, 2 * p + s, q, 0:128] for c in range(2)], axis=0)
+                    jnp.concatenate([outw[c, 2 * p + s, q] for c in range(2)], axis=0)
                     for s in range(2)
                 ],
                 axis=1,
@@ -474,27 +459,28 @@
             o_ref[:, pl.ds(pl.multiple_of(columns(g, s) * 128, 128), 128)] = total.astype(BF16)
 
     steps = (
-        (begin, UP), (in_first, 1), (in_first, 3), (pass_out,), (begin, OUT), (in_turn, 0, 3), (pass_group,),
-        (in_turn, 0, 1), (in_turn, 1, 1), (in_first_far,), (in_turn, 1, 3), (in_turn, 3, 3), (in_turn, 3, 1),
-        (turn, UP, 0, 1), (turn, UP, 0, 3), (first, OUT, 1), (in_last, 0), (in_turn, 2, 3), (in_last, 1),
-        (in_last, 3), (first, OUT, 3), (in_turn, 2, 1), (first_far, OUT), (y_group, 1), (turn, OUT, 0, 3),
-        (turn, OUT, 1, 3), (y_turn, 0, 3), (turn, OUT, 0, 1), (small_ones,), (turn, OUT, 1, 1), (y_turn, 0, 1),
-        (in_last, 2), (last, UP, 0), (y_turn, 0, 0), (turn, OUT, 3, 1), (y_turn, 0, 2), (project, 0), (y_relay,),
-        (turn, OUT, 3, 3), (small_swapped,), (turn, OUT, 2, 3), (turn, OUT, 2, 1), (last, OUT, 0), (first, UP, 1),
-        (first, UP, 3), (y_group, 2), (y_group, 3), (y_last, 1), (last, OUT, 3), (y_last, 0), (project, 1),
-        (last, OUT, 1), (begin, DOWN), (last, OUT, 2), (y_last, 2), (swapped, OUT), (project_out, 1), (y_last, 3),
-        (project, 3), (project_out, 3), (project, 2), (project_out, 2), (first_far, UP), (project_out, 0),
-        (norm_two,), (turn, UP, 3, 1), (turn, UP, 1, 1), (turn, UP, 3, 3), (turn, UP, 1, 3), (turn, UP, 2, 1),
-        (turn, UP, 2, 3), (turn, DOWN, 0, 3), (turn, DOWN, 0, 1), (last, UP, 3), (to_far_plus,), (first, DOWN, 1),
-        (to_far_minus,), (first, DOWN, 3), (last, UP, 1), (last, UP, 2), (rows_near,), (swapped, UP), (up_near,),
-        (rows_far,), (first_far, DOWN), (last, DOWN, 0), (up_far,), (swapped_row, DOWN, 0), (turn, DOWN, 1, 3),
-        (turn, DOWN, 1, 1), (down_far, 1), (down_far, 0), (up_own,), (down_near, 1), (turn, DOWN, 3, 1),
-        (down_near, 0), (pass_on, 0), (pass_on, 1), (turn, DOWN, 3, 3), (turn, DOWN, 2, 1), (turn, DOWN, 2, 3),
-        (last, DOWN, 1), (swapped_row, DOWN, 1), (down_far, 4), (down_far, 5), (down_near, 5), (finish, 1),
-        (last, DOWN, 3), (swapped_row, DOWN, 3), (down_far, 2), (down_near, 4), (last, DOWN, 2), (pass_on, 4),
-        (down_far, 3), (pass_on, 5), (swapped_row, DOWN, 2), (down_near, 6), (down_near, 3), (pass_on, 3),
-        (down_far, 6), (down_far, 7), (finish, 3), (finish, 5), (finish, 0), (down_near, 2), (finish, 4),
-        (pass_on, 6), (down_near, 7), (pass_on, 7), (pass_on, 2), (finish, 6), (finish, 7), (finish, 2),
+        (begin, UP), (in_turn, 0, 1), (in_turn, 0, 3), (in_first, 3), (pass_out,), (in_first, 1), (begin, OUT),
+        (in_last, 0), (y_turn, 0, 1), (in_turn, 3, 1), (turn, UP, 0, 1), (in_turn, 3, 3), (in_first_far,),
+        (pass_group,), (y_turn, 0, 0), (y_turn, 0, 3), (turn, UP, 0, 3), (in_turn, 1, 1), (in_turn, 1, 3),
+        (y_turn, 0, 2), (first, OUT, 3), (first, OUT, 1), (in_last, 3), (in_last, 1), (in_turn, 2, 3),
+        (in_turn, 2, 1), (first_far, OUT), (turn, OUT, 3, 1), (turn, OUT, 0, 3), (small_ones,), (turn, OUT, 3, 3),
+        (turn, OUT, 1, 3), (turn, OUT, 0, 1), (turn, OUT, 1, 1), (in_last, 2), (y_relay,), (last, UP, 0),
+        (turn, OUT, 2, 3), (y_group, 3), (turn, OUT, 2, 1), (first, UP, 1), (y_last, 0), (first, UP, 3),
+        (last, OUT, 1), (y_group, 1), (project, 0), (last, OUT, 0), (small_swapped,), (y_group, 2), (last, OUT, 3),
+        (last, OUT, 2), (project, 3), (swapped, OUT), (project_out, 3), (project_out, 0), (project, 1),
+        (first_far, UP), (y_last, 1), (y_last, 3), (project_out, 1), (y_last, 2), (project, 2), (turn, UP, 3, 1),
+        (begin, DOWN), (turn, UP, 1, 3), (project_out, 2), (norm_two,), (turn, UP, 1, 1), (turn, UP, 3, 3),
+        (turn, UP, 2, 3), (turn, DOWN, 0, 3), (turn, UP, 2, 1), (turn, DOWN, 0, 1), (last, UP, 1), (to_far_minus,),
+        (first, DOWN, 1), (to_far_plus,), (first, DOWN, 3), (last, UP, 3), (last, UP, 2), (swapped, UP),
+        (last, DOWN, 0), (up_own,), (first_far, DOWN), (rows_near,), (up_near,), (swapped_row, DOWN, 0),
+        (down_near, 0), (turn, DOWN, 1, 1), (turn, DOWN, 1, 3), (rows_far,), (up_far,), (down_far, 1),
+        (turn, DOWN, 3, 3), (down_far, 0), (turn, DOWN, 3, 1), (down_near, 1), (turn, DOWN, 2, 1),
+        (turn, DOWN, 2, 3), (pass_on, 1), (pass_on, 0), (last, DOWN, 1), (swapped_row, DOWN, 1), (down_far, 4),
+        (down_far, 5), (down_near, 4), (last, DOWN, 3), (swapped_row, DOWN, 3), (down_far, 3), (down_near, 5),
+        (down_near, 3), (finish, 1), (last, DOWN, 2), (swapped_row, DOWN, 2), (down_far, 6), (pass_on, 4),
+        (down_near, 6), (down_far, 7), (down_far, 2), (down_near, 7), (pass_on, 7), (down_near, 2), (pass_on, 2),
+        (pass_on, 6), (finish, 0), (pass_on, 5), (pass_on, 3), (finish, 7), (finish, 2), (finish, 6), (finish, 4),
+        (finish, 5), (finish, 3),
     )
     for action, *args in steps:
         action(*args)
@@ -526,14 +512,13 @@
         out_specs=vmem,
         scratch_shapes=[
             pltpu.VMEM((EXT, 2048), BF16),
-            pltpu.VMEM((2, 4, 16, HEAD, 128), BF16),
-            pltpu.VMEM((2, 16, 4, 128 + TAIL, 128), BF16),
+            pltpu.VMEM((2, 4, 16, 128, 128), BF16),
+            pltpu.VMEM((2, 16, 4, 128, 128), BF16),
             pltpu.VMEM((2, 16, 128, 1024), BF16),
             pltpu.VMEM((16, 2, 1024, 128), BF16),
             pltpu.VMEM((8, 128, 128), BF16),
             pltpu.VMEM((8, 1, 128), F32),
-            pltpu.VMEM((EXT, 16 * HEAD), BF16),
-            pltpu.VMEM((EXT, 16 * TAIL), BF16),
+            pltpu.VMEM((EXT, 2048), BF16),
             pltpu.VMEM((4, EXT, 256), F32),
             pltpu.VMEM((16, ROWS, 128), F32),
             pltpu.VMEM((4, ROWS, 256), BF16),
@@ -546,7 +531,7 @@
             pltpu.VMEM((8, 2, 64, 256), F32),
             pltpu.SemaphoreType.DMA((N_KINDS,)),
             pltpu.SemaphoreType.DMA((N_SEMS,)),
-            pltpu.SemaphoreType.DMA((8,)),
+            pltpu.SemaphoreType.DMA((7,)),
         ],
         compiler_params=pltpu.CompilerParams(
             collective_id=0, has_side_effects=True, vmem_limit_bytes=56 * 1024 * 1024

time: 89.7 us -> 88.5 us (0.987)
  Pallas kernels: 88.4 us -> 87.5 us
    pallas_call x1, Pallas kernels: 88.4 us -> 87.5 us  [local(): pl.pallas_call(kernel, out_shape=pltpu.VMEM((ROWS, 2048), BF16), in_specs...]
where the time goes in v4:
time: 88.5 us; the launch traced here: 88.3 us
  Pallas kernels  87.5 us (99%)
    pallas_call x1, Pallas kernels, local(): pl.pallas_call(kernel, out_shape=pltpu.VMEM((ROWS, 2048), BF16), in_specs...  87.5 us

profile of v4, /device:TPU:1, one launch (start us, length us, event | category | flops | bytes accessed | tf_op | source)
XLA Modules:
  0.0 88.3 jit_solution(9377058588206169644)
XLA Ops:
  0.0 87.5 %layer.1 = bf16[128,2048]{1,0:T(8,128)(2,1)S(1)} custom-call(bf16[128,2048]{1,0:T(8,128)(2,1)} %tokens_hbm.1, f32[1,2048]{1,0:T(1,128)} %bitcast.3, bf16[128,128]{1,0:T(8,128)(2,1)} %in_hbm.1, bf16[1,128,128]{2,1,0:T(8,128)(2,1)} %group_hbm.1, f32[1,128]{1,0:T(1,128)} %bitcast.5, bf16[128,128]{1,0:T(8,128)(2,1)} %out_hbm.1, f32[1,2048]{1,0:T(1,128)} %bitcast.4, ...), custom_call_target="tpu_custom_call" | custom-call | flops 10000000000 | bytes 3000000 | tf_op jit(solution)/shard_map/layer/pallas_call | solution.py:508
  87.5 0.8 copy.11

commit v5 on v4

--- a/solution.py
+++ b/solution.py
@@ -459,28 +459,27 @@
             o_ref[:, pl.ds(pl.multiple_of(columns(g, s) * 128, 128), 128)] = total.astype(BF16)
 
     steps = (
-        (begin, UP), (in_turn, 0, 1), (in_turn, 0, 3), (in_first, 3), (pass_out,), (in_first, 1), (begin, OUT),
-        (in_last, 0), (y_turn, 0, 1), (in_turn, 3, 1), (turn, UP, 0, 1), (in_turn, 3, 3), (in_first_far,),
-        (pass_group,), (y_turn, 0, 0), (y_turn, 0, 3), (turn, UP, 0, 3), (in_turn, 1, 1), (in_turn, 1, 3),
-        (y_turn, 0, 2), (first, OUT, 3), (first, OUT, 1), (in_last, 3), (in_last, 1), (in_turn, 2, 3),
-        (in_turn, 2, 1), (first_far, OUT), (turn, OUT, 3, 1), (turn, OUT, 0, 3), (small_ones,), (turn, OUT, 3, 3),
-        (turn, OUT, 1, 3), (turn, OUT, 0, 1), (turn, OUT, 1, 1), (in_last, 2), (y_relay,), (last, UP, 0),
-        (turn, OUT, 2, 3), (y_group, 3), (turn, OUT, 2, 1), (first, UP, 1), (y_last, 0), (first, UP, 3),
-        (last, OUT, 1), (y_group, 1), (project, 0), (last, OUT, 0), (small_swapped,), (y_group, 2), (last, OUT, 3),
-        (last, OUT, 2), (project, 3), (swapped, OUT), (project_out, 3), (project_out, 0), (project, 1),
-        (first_far, UP), (y_last, 1), (y_last, 3), (project_out, 1), (y_last, 2), (project, 2), (turn, UP, 3, 1),
-        (begin, DOWN), (turn, UP, 1, 3), (project_out, 2), (norm_two,), (turn, UP, 1, 1), (turn, UP, 3, 3),
-        (turn, UP, 2, 3), (turn, DOWN, 0, 3), (turn, UP, 2, 1), (turn, DOWN, 0, 1), (last, UP, 1), (to_far_minus,),
-        (first, DOWN, 1), (to_far_plus,), (first, DOWN, 3), (last, UP, 3), (last, UP, 2), (swapped, UP),
-        (last, DOWN, 0), (up_own,), (first_far, DOWN), (rows_near,), (up_near,), (swapped_row, DOWN, 0),
-        (down_near, 0), (turn, DOWN, 1, 1), (turn, DOWN, 1, 3), (rows_far,), (up_far,), (down_far, 1),
-        (turn, DOWN, 3, 3), (down_far, 0), (turn, DOWN, 3, 1), (down_near, 1), (turn, DOWN, 2, 1),
-        (turn, DOWN, 2, 3), (pass_on, 1), (pass_on, 0), (last, DOWN, 1), (swapped_row, DOWN, 1), (down_far, 4),
-        (down_far, 5), (down_near, 4), (last, DOWN, 3), (swapped_row, DOWN, 3), (down_far, 3), (down_near, 5),
-        (down_near, 3), (finish, 1), (last, DOWN, 2), (swapped_row, DOWN, 2), (down_far, 6), (pass_on, 4),
-        (down_near, 6), (down_far, 7), (down_far, 2), (down_near, 7), (pass_on, 7), (down_near, 2), (pass_on, 2),
-        (pass_on, 6), (finish, 0), (pass_on, 5), (pass_on, 3), (finish, 7), (finish, 2), (finish, 6), (finish, 4),
-        (finish, 5), (finish, 3),
+        (begin, UP), (in_turn, 0, 3), (in_first, 3), (pass_out,), (in_first, 1), (in_turn, 0, 1), (y_turn, 0, 3),
+        (pass_group,), (begin, OUT), (in_turn, 3, 1), (turn, UP, 0, 1), (in_turn, 3, 3), (in_first_far,),
+        (y_turn, 0, 0), (in_turn, 1, 1), (in_turn, 1, 3), (turn, UP, 0, 3), (in_last, 0), (y_turn, 0, 1),
+        (first, OUT, 1), (first, OUT, 3), (in_last, 3), (y_turn, 0, 2), (in_turn, 2, 1), (in_turn, 2, 3),
+        (small_ones,), (in_last, 1), (turn, OUT, 0, 3), (turn, OUT, 0, 1), (first_far, OUT), (turn, OUT, 1, 3),
+        (y_relay,), (first, UP, 1), (turn, OUT, 1, 1), (turn, OUT, 3, 3), (in_last, 2), (turn, OUT, 2, 3),
+        (project, 0), (last, OUT, 0), (y_group, 1), (turn, OUT, 3, 1), (turn, OUT, 2, 1), (first, UP, 3),
+        (y_group, 3), (y_group, 2), (y_last, 1), (y_last, 0), (last, OUT, 1), (turn, UP, 1, 3), (project, 3),
+        (first_far, UP), (project, 1), (last, OUT, 3), (y_last, 2), (small_swapped,), (last, OUT, 2), (y_last, 3),
+        (begin, DOWN), (swapped, OUT), (project_out, 0), (project, 2), (project_out, 3), (project_out, 1),
+        (project_out, 2), (norm_two,), (last, UP, 0), (turn, UP, 3, 3), (turn, UP, 3, 1), (turn, UP, 1, 1),
+        (turn, UP, 2, 3), (turn, UP, 2, 1), (to_far_plus,), (turn, DOWN, 0, 1), (to_far_minus,), (turn, DOWN, 0, 3),
+        (first, DOWN, 1), (first, DOWN, 3), (last, UP, 1), (last, UP, 2), (last, UP, 3), (swapped, UP), (up_own,),
+        (last, DOWN, 0), (first_far, DOWN), (rows_near,), (up_near,), (swapped_row, DOWN, 0), (turn, DOWN, 1, 3),
+        (rows_far,), (up_far,), (turn, DOWN, 1, 1), (down_far, 1), (down_far, 0), (turn, DOWN, 3, 3),
+        (turn, DOWN, 3, 1), (down_near, 0), (down_near, 1), (turn, DOWN, 2, 1), (pass_on, 1), (turn, DOWN, 2, 3),
+        (pass_on, 0), (last, DOWN, 1), (swapped_row, DOWN, 1), (down_far, 5), (down_far, 4), (down_near, 5),
+        (last, DOWN, 3), (swapped_row, DOWN, 3), (down_far, 2), (down_near, 3), (down_far, 3), (last, DOWN, 2),
+        (swapped_row, DOWN, 2), (down_near, 7), (pass_on, 5), (down_far, 6), (down_far, 7), (down_near, 6),
+        (finish, 0), (down_near, 4), (pass_on, 3), (pass_on, 4), (down_near, 2), (finish, 5), (pass_on, 2),
+        (pass_on, 7), (pass_on, 6), (finish, 3), (finish, 4), (finish, 7), (finish, 2), (finish, 1), (finish, 6),
     )
     for action, *args in steps:
         action(*args)

time: 88.5 us -> 86.4 us (0.976)
  Pallas kernels: 87.5 us -> 85.4 us
    pallas_call x1, Pallas kernels: 87.5 us -> 85.4 us  [local(): pl.pallas_call(kernel, out_shape=pltpu.VMEM((ROWS, 2048), BF16), in_specs...]
where the time goes in v5:
time: 86.4 us; the launch traced here: 86.2 us
  Pallas kernels  85.4 us (99%)
    pallas_call x1, Pallas kernels, local(): pl.pallas_call(kernel, out_shape=pltpu.VMEM((ROWS, 2048), BF16), in_specs...  85.4 us

profile of v5, /device:TPU:1, one launch (start us, length us, event | category | flops | bytes accessed | tf_op | source)
XLA Modules:
  0.0 86.2 jit_solution(8107054509692210719)
XLA Ops:
  0.0 85.4 %layer.1 = bf16[128,2048]{1,0:T(8,128)(2,1)S(1)} custom-call(bf16[128,2048]{1,0:T(8,128)(2,1)} %tokens_hbm.1, f32[1,2048]{1,0:T(1,128)} %bitcast.3, bf16[128,128]{1,0:T(8,128)(2,1)} %in_hbm.1, bf16[1,128,128]{2,1,0:T(8,128)(2,1)} %group_hbm.1, f32[1,128]{1,0:T(1,128)} %bitcast.5, bf16[128,128]{1,0:T(8,128)(2,1)} %out_hbm.1, f32[1,2048]{1,0:T(1,128)} %bitcast.4, ...), custom_call_target="tpu_custom_call" | custom-call | flops 10000000000 | bytes 3000000 | tf_op jit(solution)/shard_map/layer/pallas_call | solution.py:507
  85.4 0.8 copy.11
